TPU v7x, 32 devices: a whole 2x2x4 slice. The times are simulated.
32 devices in a mesh: sp: 4 (over z), fs: 4 (over y, x), tp: 2 (over core).
Axes of the slice: x: 2, y: 2, z: 4, core: 2. Of those that a mesh axis runs over, the one named last changes fastest.
Arguments:
- inputs: bfloat16 [4, 512, 2048], P('fs', 'sp', 'tp'), may hold values from -1000 to 1000
- input_norm_gain: float32 [2048], replicated, may hold values from 0.1 to 1.9
- receptance_weight: bfloat16 [2048, 1024], P(('sp', 'fs'), 'tp'), may hold values from -0.125 to 0.125
- linear_key_weight: bfloat16 [2048, 1024], P(('sp', 'fs'), 'tp'), may hold values from -0.125 to 0.125
- linear_value_weight: bfloat16 [2048, 1024], P(('sp', 'fs'), 'tp'), may hold values from -0.125 to 0.125
- window_query_weight: bfloat16 [2048, 1024], P(('sp', 'fs'), 'tp'), may hold values from -1 to 1
- window_key_weight: bfloat16 [2048, 256], P(('sp', 'fs'), 'tp'), may hold values from -1 to 1
- window_value_weight: bfloat16 [2048, 256], P(('sp', 'fs'), 'tp'), may hold values from -0.125 to 0.125
- decay_down_weight: bfloat16 [2048, 96], replicated, may hold values from -0.125 to 0.125
- decay_up_weight: bfloat16 [2, 96, 1024], replicated, may hold values from -1 to 1
- decay_offset: float32 [2, 1024], replicated, may hold values from -13 to -3
- decay_log_extra: float32 [4, 16, 512], P('fs', 'tp', 'sp'), may hold values from -1.4 to 0
- erasure_down_weight: bfloat16 [2048, 96], replicated, may hold values from -0.125 to 0.125
- erasure_up_weight: bfloat16 [2, 96, 1024], replicated, may hold values from -0.625 to 0.625
- erasure_offset: float32 [2, 1024], replicated, may hold values from -9.5 to 1
- initial_state: float32 [2, 16, 64, 64], replicated, may hold values from -128 to 128
- head_norm_gain: float32 [1024], replicated, may hold values from 0.1 to 1.9
- query_sink_logit: float32 [16], replicated, may hold values from 2 to 7
- linear_output_weight: bfloat16 [1024, 2048], P('tp', ('sp', 'fs')), may hold values from -0.1875 to 0.1875
- window_output_weight: bfloat16 [1024, 2048], P('tp', ('sp', 'fs')), may hold values from -1.5 to 1.5
Outputs:
- layer_out: bfloat16 [4, 512, 2048], P('fs', ('sp', 'tp'))
All inputs are finite; a program needn't handle non-finite values.
Results may differ from a plain program's by a relative error of at most 0.006.
The roundings to bfloat16 on the way count: a program that leaves them out, or rounds other values in their place, can miss the bound.
Values may be sent and summed in bfloat16 or wider, within the bound.
A program may use at most 128 MiB of HBM per device.

v0:
```python
import jax
import jax.numpy as jnp
from jax import lax
from jax.experimental import pallas as pl
from jax.experimental.pallas import tpu as pltpu
from jax.sharding import PartitionSpec as P

HD = 64
WINDOW = 128
GRID_W = 64
ATT_BLOCK = 128


NORM_EPS = 1e-06
GROUP_EPS = 0.00064
ROPE_BASE = 10000.0
HIGHEST = lax.Precision.HIGHEST


def padded(block, sides, width):
    for axis, dim in sides:
        count = lax.axis_size(axis)
        forward = [(i, i + 1) for i in range(count - 1)]
        backward = [(target, source) for source, target in forward]
        low = lax.ppermute(
            lax.slice_in_dim(block, block.shape[dim] - width, None, axis=dim), axis, forward
        )
        high = lax.ppermute(lax.slice_in_dim(block, 0, width, axis=dim), axis, backward)
        block = jnp.concatenate([low, block, high], axis=dim)
    return block


def to_bf16(array):
    return lax.optimization_barrier(array.astype(jnp.bfloat16))


def rope_axial(values, positions):
    quarter = values.shape[-1] // 4
    inverse = ROPE_BASE ** (-jnp.arange(quarter, dtype=jnp.float32) / quarter)
    grid_rows = (positions // GRID_W).astype(jnp.float32)
    grid_cols = (positions % GRID_W).astype(jnp.float32)
    pieces = []
    for which_half, coordinate in ((0, grid_rows), (1, grid_cols)):
        angles = coordinate[:, None] * inverse[None, :]
        cosine = jnp.cos(angles)[:, None, :]
        sine_part = jnp.sin(angles)[:, None, :]
        front_part = values[..., 2 * which_half * quarter : (2 * which_half + 1) * quarter]
        back_part = values[..., (2 * which_half + 1) * quarter : (2 * which_half + 2) * quarter]
        pieces.append(front_part * cosine - back_part * sine_part)
        pieces.append(front_part * sine_part + back_part * cosine)
    return jnp.concatenate(pieces, axis=-1)


CHUNK = 32
PAIR = 2 * HD
F32 = jnp.float32
NN = (((1,), (0,)), ((), ()))
NT = (((1,), (1,)), ((), ()))


def dot1(left, right, dims=NN):
    return lax.dot_general(
        left.astype(jnp.bfloat16), right.astype(jnp.bfloat16), dims, preferred_element_type=F32
    )


def halves(value):
    high = value.astype(jnp.bfloat16)
    return high, (value - high.astype(F32)).astype(jnp.bfloat16)


def dot3(left, right, dims=NN):
    left_high, left_low = halves(left)
    right_high, right_low = halves(right)

    def product(one, other):
        return lax.dot_general(one, other, dims, preferred_element_type=F32)

    return product(left_high, right_high) + (
        product(left_high, right_low) + product(left_low, right_high)
    )


def full_dot(left, right):
    return lax.dot_general(left, right, NN, precision=HIGHEST, preferred_element_type=F32)


def chunk_kernel(read_ref, key_ref, value_ref, log_ref, learn_ref, out_ref, end_ref):
    tokens = read_ref.shape[0]
    read = read_ref[...].astype(F32)
    key = key_ref[...].astype(F32)
    value = value_ref[...].astype(F32)
    first = lax.broadcasted_iota(jnp.int32, (tokens, PAIR), 1) < HD
    pair_i = lax.broadcasted_iota(jnp.int32, (PAIR, PAIR), 0)
    pair_j = lax.broadcasted_iota(jnp.int32, (PAIR, PAIR), 1)
    same_head = jnp.where(pair_i // HD == pair_j // HD, 1.0, 0.0)
    row = lax.broadcasted_iota(jnp.int32, (tokens, tokens), 0)
    col = lax.broadcasted_iota(jnp.int32, (tokens, tokens), 1)
    same_chunk = row // CHUNK == col // CHUNK
    eye = jnp.where(row == col, 1.0, 0.0)
    unit = key * lax.rsqrt(full_dot(key * key, same_head) + NORM_EPS)
    own = (first, jnp.logical_not(first))
    values = (
        jnp.where(first, value, 0.0),
        jnp.where(first, pltpu.roll(value, HD, 1), 0.0),
    )
    all_chunk = jnp.where(same_chunk, 1.0, 0.0)
    for direction in range(2):
        before = (col < row) if direction == 0 else (col > row)
        strict = same_chunk & before
        upto = same_chunk & (before | (col == row))
        log_decay = log_ref[direction]
        erase = unit * learn_ref[direction]
        total_log = full_dot(jnp.where(upto, 1.0, 0.0), log_decay)
        chunk_log = full_dot(all_chunk, log_decay)
        prior_log = total_log - log_decay
        middle = 0.5 * chunk_log
        unit_start = jnp.exp(prior_log) * unit
        unit_mid = jnp.exp(prior_log - middle) * unit
        read_start = jnp.exp(total_log) * read
        read_mid = jnp.exp(total_log - middle) * read
        inverse = jnp.exp(middle - total_log)
        sources = jnp.concatenate([erase * inverse, key * inverse], axis=0)
        rest = jnp.exp(chunk_log - total_log)
        key_rest = key * rest
        erase_rest = erase * rest
        chunk_decay = jnp.exp(chunk_log).T
        solved, offsets, mixes = [], [], []
        for head in range(2):
            readers = jnp.concatenate(
                [jnp.where(own[head], unit_mid, 0.0), jnp.where(own[head], read_mid, 0.0)], axis=0
            )
            meets = dot3(readers, sources, NT)
            erased = jnp.where(strict, meets[:tokens, :tokens], 0.0)
            seen = jnp.where(strict, meets[:tokens, tokens:], 0.0)
            read_erased = jnp.where(upto, meets[tokens:, :tokens], 0.0)
            read_seen = jnp.where(upto, meets[tokens:, tokens:], 0.0)
            solve = eye - jnp.where(row // 2 == col // 2, erased, 0.0)
            size = 2
            while size < CHUNK:
                level = (row // (2 * size) == col // (2 * size)) & (row // size != col // size)
                solve = solve - dot1(dot1(solve, jnp.where(level, erased, 0.0)), solve)
                size *= 2
            solve = solve + dot1(solve, eye - solve - dot3(erased, solve))
            both = dot3(
                solve,
                jnp.concatenate(
                    [jnp.where(own[head], unit_start, 0.0), dot3(seen, values[head])], axis=1
                ),
            )
            solved.append(both[:, :PAIR])
            offsets.append(both[:, PAIR:])
            mixes.append(jnp.concatenate([read_seen, -read_erased], axis=1))
        state = jnp.where(pair_j == HD + pair_i % HD, 1.0, 0.0)
        count = tokens // CHUNK
        drops = [[None] * count, [None] * count]
        reads = [[None] * count, [None] * count]
        for step in range(count):
            place = step if direction == 0 else count - 1 - step
            rows = slice(place * CHUNK, (place + 1) * CHUNK)
            lefts = jnp.concatenate(
                [solved[0][rows], solved[1][rows]]
                + [jnp.where(own[head], read_start, 0.0)[rows] for head in range(2)],
                axis=0,
            )
            seen_state = dot3(lefts, state)
            for head in range(2):
                drops[head][place] = (
                    seen_state[head * CHUNK : (head + 1) * CHUNK] + offsets[head][rows]
                )
                reads[head][place] = seen_state[(2 + head) * CHUNK : (3 + head) * CHUNK]
            adders = jnp.concatenate(
                [jnp.where(own[head], key_rest, 0.0)[rows] for head in range(2)]
                + [jnp.where(own[head], -erase_rest, 0.0)[rows] for head in range(2)],
                axis=0,
            ).T
            added = jnp.concatenate(
                [values[0][rows], values[1][rows], drops[0][place], drops[1][place]], axis=0
            )
            first_col = place * CHUNK
            state = chunk_decay[:, first_col : first_col + 1] * state + dot3(adders, added)
        for head in range(2):
            dropped = jnp.concatenate(drops[head], axis=0)
            out_ref[direction, head] = jnp.concatenate(reads[head], axis=0) + dot3(
                mixes[head], jnp.concatenate([values[head], dropped], axis=0)
            )
        end_ref[direction] = state


def chunked(returned, log_decay, learn, head_width):
    tokens = returned.shape[0]
    pairs = head_width // PAIR

    def role(which):
        return pl.BlockSpec((tokens, PAIR), lambda p: (0, which * pairs + p))

    wide = pl.BlockSpec((2, tokens, PAIR), lambda p: (0, 0, p))
    return pl.pallas_call(
        chunk_kernel,
        grid=(pairs,),
        in_specs=[role(0), role(1), role(2), wide, wide],
        out_specs=[
            pl.BlockSpec((2, 2, tokens, PAIR), lambda p: (0, p, 0, 0)),
            pl.BlockSpec((2, PAIR, PAIR), lambda p: (0, p, 0)),
        ],
        out_shape=[
            jax.ShapeDtypeStruct((2, 2 * pairs, tokens, PAIR), F32),
            jax.ShapeDtypeStruct((2, pairs * PAIR, PAIR), F32),
        ],
        cost_estimate=pl.CostEstimate(
            flops=pairs * 400 * PAIR**3, bytes_accessed=8 * tokens * head_width * 4, transcendentals=0
        ),
        name="chunked_state",
    )(returned, returned, returned, log_decay, learn)


def merge_kernel(local_ref, state_ref, gain_ref, out_ref):
    pair_i = lax.broadcasted_iota(jnp.int32, (PAIR, PAIR), 0)
    pair_j = lax.broadcasted_iota(jnp.int32, (PAIR, PAIR), 1)
    average = jnp.where(pair_i // HD == pair_j // HD, 1.0 / HD, 0.0)
    sums = []
    for head in range(2):
        total = 0.0
        for direction in range(2):
            block = local_ref[direction, head]
            total = total + (
                block[:, :HD] + dot3(block[:, HD:], state_ref[direction, head])
            )
        sums.append(total)
    lin_sum = jnp.concatenate(sums, axis=1)
    centred = lin_sum - full_dot(lin_sum, average)
    normed = centred * lax.rsqrt(full_dot(centred * centred, average) + GROUP_EPS)
    out_ref[...] = (normed * gain_ref[...]).astype(jnp.bfloat16)


def merged(local_out, entry, gain):
    _, head_count, tokens, _ = local_out.shape
    pairs = head_count // 2
    return pl.pallas_call(
        merge_kernel,
        grid=(pairs,),
        in_specs=[
            pl.BlockSpec((2, 2, tokens, PAIR), lambda p: (0, p, 0, 0)),
            pl.BlockSpec((2, 2, HD, HD), lambda p: (0, p, 0, 0)),
            pl.BlockSpec((1, PAIR), lambda p: (0, p)),
        ],
        out_specs=pl.BlockSpec((tokens, PAIR), lambda p: (0, p)),
        out_shape=jax.ShapeDtypeStruct((tokens, head_count * HD), jnp.bfloat16),
        cost_estimate=pl.CostEstimate(
            flops=pairs * 30 * PAIR**3, bytes_accessed=4 * tokens * head_count * PAIR * 4, transcendentals=0
        ),
        name="merged_norm",
    )(local_out, entry, gain[None, :])


def entering_states(ends, initial):
    count = lax.axis_size("sp")
    place = lax.axis_index("sp")
    ups = [(i, i + 1) for i in range(count - 1)]
    downs = [(i + 1, i) for i in range(count - 1)]
    adds, maps = ends[..., :HD], ends[..., HD:]

    def hop(_, states):
        later = jnp.einsum("dhkj,dhjv->dhkv", maps, states, precision=HIGHEST) + adds
        forward = lax.ppermute(later[0], "sp", ups)
        backward = lax.ppermute(later[1], "sp", downs)
        return jnp.stack(
            [
                jnp.where(place == 0, initial[0], forward),
                jnp.where(place == count - 1, initial[1], backward),
            ]
        )

    states = initial
    if count > 8:
        return lax.fori_loop(0, count - 1, hop, states)
    for _ in range(count - 1):
        states = hop(0, states)
    return states


def swapped(block, axis):
    count = lax.axis_size(axis)
    return [block] + [
        lax.ppermute(block, axis, [(i, i ^ flip) for i in range(count)]) for flip in range(1, count)
    ]


def in_order(pieces, axis):
    me = lax.axis_index(axis)
    stacked = jnp.stack(pieces)
    return [
        lax.dynamic_index_in_dim(stacked, me ^ place, 0, False) for place in range(len(pieces))
    ]


def local(
    inputs,
    input_norm_gain,
    receptance_weight,
    linear_key_weight,
    linear_value_weight,
    window_query_weight,
    window_key_weight,
    window_value_weight,
    decay_down_weight,
    decay_up_weight,
    decay_offset,
    decay_log_extra,
    erasure_down_weight,
    erasure_up_weight,
    erasure_offset,
    initial_state,
    head_norm_gain,
    query_sink_logit,
    linear_output_weight,
    window_output_weight,
):
    tokens = inputs.shape[1]
    tp_index = lax.axis_index("tp")
    length = tokens * lax.axis_size("sp")
    offset = lax.axis_index("sp") * tokens
    gathered = lax.all_gather(inputs, "tp", axis=2, tiled=True)[0]
    widened = gathered.astype(jnp.float32)
    hidden = to_bf16(
        widened
        * lax.rsqrt(jnp.mean(widened * widened, axis=-1, keepdims=True) + NORM_EPS)
        * input_norm_gain
    )
    weights = (
        receptance_weight,
        linear_key_weight,
        linear_value_weight,
        window_query_weight,
        window_key_weight,
        window_value_weight,
    )
    widths = [weight.shape[1] for weight in weights]
    joined = jnp.concatenate(weights, axis=1)
    regrouped = lax.all_to_all(joined, "fs", split_axis=1, concat_axis=0, tiled=True)
    every_seq = jnp.concatenate(swapped(hidden, "fs"), axis=0)
    near_cols = jnp.concatenate(in_order(swapped(window_output_weight, "fs"), "fs"), axis=1)
    whole_cols = lax.all_gather(regrouped, "sp", axis=0, tiled=True)
    partial_cols = jnp.dot(every_seq, whole_cols, preferred_element_type=jnp.float32)
    by_seq = to_bf16(partial_cols).reshape(-1, tokens, partial_cols.shape[1])
    outgoing = jnp.concatenate(in_order(list(by_seq), "fs"), axis=0)
    returned = lax.all_to_all(outgoing, "fs", split_axis=0, concat_axis=1, tiled=True)
    bounds = [0]
    for col_width in widths:
        bounds.append(bounds[-1] + col_width)
    projected = [returned[:, bounds[role_idx] : bounds[role_idx + 1]] for role_idx in range(6)]
    recept, lin_keys, lin_values, queries, att_keys, att_values = projected
    head_width = recept.shape[1]
    head_count = head_width // HD
    first_col = tp_index * head_width
    up_decay = lax.dynamic_slice_in_dim(decay_up_weight, first_col, head_width, 2)
    up_learn = lax.dynamic_slice_in_dim(erasure_up_weight, first_col, head_width, 2)
    base_decay = lax.dynamic_slice_in_dim(decay_offset, first_col, head_width, 1)
    base_learn = lax.dynamic_slice_in_dim(erasure_offset, first_col, head_width, 1)
    gain_local = lax.dynamic_slice_in_dim(head_norm_gain, first_col, head_width, 0)
    state_local = lax.dynamic_slice_in_dim(initial_state, tp_index * head_count, head_count, 1)
    spread = (
        jnp.arange(head_count)[:, None] == jnp.arange(head_width)[None, :] // HD
    ).astype(jnp.float32)
    decay_spikes = jnp.einsum("ht,hc->tc", decay_log_extra[0], spread, precision=HIGHEST)
    decay_low = to_bf16(jnp.dot(hidden, decay_down_weight, preferred_element_type=jnp.float32))
    decay_act = to_bf16(jnp.tanh(decay_low.astype(jnp.float32)))
    learn_low = to_bf16(jnp.dot(hidden, erasure_down_weight, preferred_element_type=jnp.float32))
    pre_decay = base_decay[:, None, :] + jnp.einsum(
        "tl,dlc->dtc", decay_act, up_decay, preferred_element_type=jnp.float32
    )
    log_decay = decay_spikes[None] - jnp.exp(-jax.nn.softplus(-pre_decay) - 0.5)
    learn = jax.nn.sigmoid(
        base_learn[:, None, :]
        + jnp.einsum("tl,dlc->dtc", learn_low, up_learn, preferred_element_type=jnp.float32)
    )
    local_out, ends = chunked(returned, log_decay, learn, head_width)
    entry = entering_states(
        ends.reshape(2, head_count, HD, PAIR), jnp.swapaxes(state_local, -1, -2)
    )
    lin_mix = merged(local_out, entry, gain_local)
    positions = offset + jnp.arange(tokens, dtype=jnp.int32)
    query_count = queries.shape[1] // HD
    group_count = att_keys.shape[1] // HD
    group_size = query_count // group_count
    roped_q = rope_axial(
        queries.astype(jnp.float32).reshape(tokens, query_count, HD), positions
    ).astype(jnp.bfloat16)
    roped_k = rope_axial(
        att_keys.astype(jnp.float32).reshape(tokens, group_count, HD), positions
    ).astype(jnp.bfloat16)
    kv_width = group_count * HD
    packed = jnp.concatenate([roped_k.reshape(tokens, kv_width), att_values], axis=1)
    bordered = padded(packed, (("sp", 0),), WINDOW)
    sink_local = lax.dynamic_slice_in_dim(
        query_sink_logit, tp_index * query_count, query_count, 0
    ).reshape(group_count, group_size)[:, :, None, None]
    reach = ATT_BLOCK + 2 * WINDOW
    query_rows = roped_q.reshape(ATT_BLOCK, group_count, group_size, HD)
    key_rows = bordered[:, :kv_width].reshape(reach, group_count, HD)
    value_rows = bordered[:, kv_width:].reshape(reach, group_count, HD)
    scores = jnp.einsum(
        "qgrd,kgd->grqk", query_rows, key_rows, preferred_element_type=jnp.float32
    ) * HD ** (-0.5)
    query_pos = offset + 0 + jnp.arange(ATT_BLOCK, dtype=jnp.int32)
    key_pos = offset + 0 - WINDOW + jnp.arange(reach, dtype=jnp.int32)
    allowed = (
        (jnp.abs(query_pos[:, None] - key_pos[None, :]) <= WINDOW)
        & (key_pos[None, :] >= 0)
        & (key_pos[None, :] < length)
    )
    scores = jnp.where(allowed, scores, -jnp.inf)
    top_score = jnp.maximum(jnp.max(scores, axis=-1, keepdims=True), sink_local)
    raised = jnp.exp(scores - top_score)
    denominator = jnp.exp(sink_local - top_score) + jnp.sum(raised, axis=-1, keepdims=True)
    weights_bf = (raised / denominator).astype(jnp.bfloat16)
    mixed = jnp.einsum("grqk,kgd->qgrd", weights_bf, value_rows, preferred_element_type=jnp.float32)
    outputs = mixed.astype(jnp.bfloat16).reshape(ATT_BLOCK, query_count * HD)
    lin_weight = lax.all_gather(linear_output_weight, ("sp", "fs"), axis=1, tiled=True)
    if lax.axis_size("sp") > 8:
        att_out = jnp.dot(
            outputs,
            lax.all_gather(near_cols, "sp", axis=1, tiled=True),
            preferred_element_type=jnp.float32,
        )
    else:
        att_parts = [
            jnp.dot(outputs, part, preferred_element_type=jnp.float32)
            for part in swapped(near_cols, "sp")
        ]
        att_out = jnp.concatenate(in_order(att_parts, "sp"), axis=1)
    layer_out = lax.psum_scatter(
        jnp.dot(lin_mix, lin_weight, preferred_element_type=jnp.float32) + att_out,
        "tp",
        scatter_dimension=0,
        tiled=True,
    )
    return layer_out.astype(jnp.bfloat16)[None]


def solution(mesh):
    return jax.shard_map(
        local,
        mesh=mesh,
        in_specs=(
            P("fs", "sp", "tp"),
            P(),
            P(("sp", "fs"), "tp"),
            P(("sp", "fs"), "tp"),
            P(("sp", "fs"), "tp"),
            P(("sp", "fs"), "tp"),
            P(("sp", "fs"), "tp"),
            P(("sp", "fs"), "tp"),
            P(),
            P(),
            P(),
            P("fs", "tp", "sp"),
            P(),
            P(),
            P(),
            P(),
            P(),
            P(),
            P("tp", ("sp", "fs")),
            P("tp", ("sp", "fs")),
        ),
        out_specs=P("fs", ("sp", "tp"), None),
        check_vma=False,
    )
```

profile of v0, /device:TPU:0, one launch (start us, length us, event | category | flops | bytes accessed | tf_op | source)
XLA Modules:
  0.0 218.8 jit_solution(2589721792258808189)
XLA Ops:
  6.5 1.1 copy.50
  7.7 1.0 copy.51
  8.7 1.0 copy.52
  9.7 1.0 copy.53
  10.8 0.9 copy.54
  11.6 0.9 copy.55
  12.6 14.5 %all_to_all.38 = bf16[128,4,576]{0,2,1:T(8,128)(2,1)S(1)} all-to-all(bf16[128,4,576]{0,2,1:T(8,128)(2,1)S(1)} %bitcast.179), channel_id=1, replica_groups=mesh['sp'=4,'fs'=4,'tp'=2] {'fs'}, dimensions={1} | all-to-all | bytes 1179648 | tf_op jit(solution)/shard_map/all_to_all | solution.py:340
  27.2 0.9 copy_bitcast_fusion
  28.2 2.3 %all_gather.9 = bf16[1,128,2048]{2,1,0:T(8,128)(2,1)S(1)} all-gather(bf16[1,128,1024]{2,1,0:T(8,128)(2,1)S(1)} %copy-done.10), channel_id=1, replica_groups=mesh['sp'=4,'fs'=4,'tp'=2] {'tp'}, dimensions={2}, use_global_device_ids=true | all-gather | bytes 786432 | tf_op jit(solution)/shard_map/all_gather | solution.py:323
  31.7 1.5 collective-permute-start.1
  33.2 1.3 collective-permute-start
  35.2 1.5 collective-permute-start.12
  39.1 2.1 fusion.18.learn_ref
  41.2 2.3 %fusion.25.log_ref = f32[2,128,512]{2,1,0:T(8,128)} fusion(f32[2,512]{1,0:T(2,128)S(1)} %get-tuple-element.64, f32[128,512]{1,0:T(8,128)S(1)} %copy.58, bf16[2,96,1024]{2,1,0:T(8,128)(2,1)} %param.29, s32[]{:T(128)S(6)} %select_n.118, bf16[128,96]{0,1:T(8,128)(2,1)S(1)} %tanh_convert_fusion), kind=kOutput, calls=%fused_computation.48 | convolution fusion | flops 26607616 | bytes 1011716 | tf_op jit(solution)/shard_map/tl,dlc->dtc/dot_general | solution.py:369
  43.5 3.2 %collective-permute-done.2 = bf16[128,2048]{1,0:T(8,128)(2,1)S(1)} collective-permute-done((bf16[128,2048]{1,0:T(8,128)(2,1)S(1)}, bf16[128,2048]{1,0:T(8,128)(2,1)S(1)}, u32[]{:S(2)}, u32[]{:S(2)}) %collective-permute-start.2) | collective-permute-done | bytes 524320 | tf_op jit(solution)/shard_map/ppermute | solution.py:285
  47.5 10.7 %collective-permute-done.1 = bf16[128,2048]{1,0:T(8,128)(2,1)} collective-permute-done((bf16[128,2048]{1,0:T(8,128)(2,1)S(1)}, bf16[128,2048]{1,0:T(8,128)(2,1)}, u32[]{:S(2)}, u32[]{:S(2)}) %collective-permute-start.1) | collective-permute-done | bytes 524320 | tf_op jit(solution)/shard_map/ppermute | solution.py:285
  58.1 19.7 %all-gather.3.cloned.1.call-done = bf16[2048,576]{0,1:T(8,128)(2,1)} async-done(((bf16[512,576]{0,1:T(8,128)(2,1)}), bf16[2048,576]{0,1:T(8,128)(2,1)}) %all-gather.3.cloned.1.call-update) | async-done | bytes 2359312 | tf_op jit(solution)/shard_map/all_gather | solution.py:343
  77.9 3.4 %fusion.9 = bf16[512,576]{0,1:T(8,128)(2,1)S(1)} fusion(bf16[2048,576]{0,1:T(8,128)(2,1)} %all-gather.3.cloned.1.call-done, bf16[128,2048]{1,0:T(8,128)(2,1)S(1)} %collective-permute-done.2, bf16[128,2048]{1,0:T(8,128)(2,1)} %collective-permute-done.1, bf16[128,2048]{1,0:T(8,128)(2,1)} %collective-permute-done, bf16[128,2048]{1,0:T(8,128)(2,1)S(1)} %fusion.21), kind=kOutput, calls=%fused_computation.14 | convolution fusion | flops 1216643072 | bytes 5046272 | tf_op jit(solution)/shard_map/dot_general | solution.py:344
  81.5 0.9 copy_bitcast_fusion.1
  82.4 3.7 %all-to-all-start.1 = ((bf16[4,128,576]{1,2,0:T(8,128)(2,1)}), bf16[4,128,576]{1,2,0:T(8,128)(2,1)S(1)}, u32[]{:S(2)}, u32[]{:S(2)}) async-start(bf16[4,128,576]{1,2,0:T(8,128)(2,1)} %copy_bitcast_fusion.1), calls=%async_computation.1 | async-start | bytes 1179648 | tf_op jit(solution)/shard_map/all_to_all | solution.py:347
  87.7 1.0 pad_maximum_fusion.3
  88.8 0.9 pad_maximum_fusion.4
  89.7 1.2 collective-permute-start.16
  91.1 3.0 %collective-permute-start.14 = (bf16[512,512]{1,0:T(8,128)(2,1)}, bf16[512,512]{1,0:T(8,128)(2,1)S(1)}, u32[]{:S(2)}, u32[]{:S(2)}) collective-permute-start(bf16[512,512]{1,0:T(8,128)(2,1)} %pad_maximum_fusion.4), channel_id=1, source_target_pairs={{0,8},{8,0},{16,24},{24,16},{1,9},{9,1},{17,25},{25,17},{2,10},{10... | collective-permute-start | bytes 1572872 | tf_op jit(solution)/shard_map/ppermute | solution.py:285
  94.1 2.2 %all-to-all-done.1 = bf16[4,128,576]{1,2,0:T(8,128)(2,1)S(1)} async-done(((bf16[4,128,576]{1,2,0:T(8,128)(2,1)}), bf16[4,128,576]{1,2,0:T(8,128)(2,1)S(1)}, u32[]{:S(2)}, u32[]{:S(2)}) %all-to-all-start.1) | async-done | bytes 589856 | tf_op jit(solution)/shard_map/all_to_all | solution.py:347
  96.3 1.1 copy.61.read_ref.key_ref.value_ref
  98.1 1.3 collective-permute-start.10
  99.4 5.2 %collective-permute-start.9 = (bf16[128,256]{0,1:T(8,128)(2,1)}, bf16[128,256]{0,1:T(8,128)(2,1)}, u32[]{:S(2)}, u32[]{:S(2)}) collective-permute-start(bf16[128,256]{0,1:T(8,128)(2,1)} %pad_maximum_fusion.6), channel_id=1, source_target_pairs={{0,8},{8,16},{16,24},{1,9},{9,17},{17,25},{2,10},{10,18},{18,26},{... | collective-permute-start | bytes 196616 | tf_op jit(solution)/shard_map/ppermute | solution.py:25
  104.6 41.7 %chunked_state.1 = (f32[2,8,128,128]{3,2,1,0:T(8,128)}, f32[2,512,128]{2,1,0:T(8,128)}) custom-call(bf16[128,2304]{1,0:T(8,128)(2,1)} %copy.61.read_ref.key_ref.value_ref, bf16[128,2304]{1,0:T(8,128)(2,1)} %copy.61.read_ref.key_ref.value_ref, bf16[128,2304]{1,0:T(8,128)(2,1)} %copy.61.read_ref.key_ref.value_ref, f32[2,128,512]{2,1,0:T(8,128)} %fusion.25.log_ref, ...), custom_call_target="tpu_custom_call" | custom-call | flops 3355443200 | bytes 2097152 | tf_op jit(solution)/shard_map/chunked_state/pallas_call | solution.py:198
  146.4 2.2 %convolution_add_fusion.3 = f32[2,8,64,64]{3,2,1,0:T(8,128)S(1)} fusion(f32[2,8,64,64]{3,2,1,0:T(8,128)S(1)} %constant_dynamic-slice_fusion, f32[2,8,64,128]{3,2,1,0:T(8,128)} %bitcast.169), kind=kOutput, calls=%fused_computation.19 | convolution fusion | flops 50397184 | bytes 1572864 | tf_op jit(solution)/shard_map/dhkj,dhjv->dhkv/dot_general | solution.py:264
  148.8 11.2 %collective-permute-start.3 = (f32[8,64,64]{2,1,0:T(8,128)S(1)}, f32[8,64,64]{2,1,0:T(8,128)S(1)}, u32[]{:S(2)}, u32[]{:S(2)}) collective-permute-start(f32[8,64,64]{2,1,0:T(8,128)S(1)} %get-tuple-element.37), channel_id=1, source_target_pairs={{0,8},{8,16},{16,24},{1,9},{9,17},{17,25},{2,10},{10,18},{18,26},{... | collective-permute-start | bytes 393224 | tf_op jit(solution)/shard_map/ppermute | solution.py:265
  160.0 1.5 collective-permute-start.4
  161.5 0.9 pad_maximum_fusion.5
  163.7 1.4 convolution_bitcast_fusion
  165.1 1.3 convolution_bitcast_fusion.1
  167.0 1.6 collective-permute-done.4
  169.4 4.4 %collective-permute-start.5 = (f32[8,64,64]{2,1,0:T(8,128)S(1)}, f32[8,64,64]{2,1,0:T(8,128)S(1)}, u32[]{:S(2)}, u32[]{:S(2)}) collective-permute-start(f32[8,64,64]{2,1,0:T(8,128)S(1)} %get-tuple-element.33), channel_id=1, source_target_pairs={{0,8},{8,16},{16,24},{1,9},{9,17},{17,25},{2,10},{10,18},{18,26},{... | collective-permute-start | bytes 393224 | tf_op jit(solution)/shard_map/ppermute | solution.py:265
  173.8 1.3 collective-permute-start.6
  175.2 2.5 %collective-permute-done.5 = f32[8,64,64]{2,1,0:T(8,128)S(1)} collective-permute-done((f32[8,64,64]{2,1,0:T(8,128)S(1)}, f32[8,64,64]{2,1,0:T(8,128)S(1)}, u32[]{:S(2)}, u32[]{:S(2)}) %collective-permute-start.5) | collective-permute-done | bytes 131104 | tf_op jit(solution)/shard_map/ppermute | solution.py:265
  177.6 4.4 %collective-permute-done.6 = f32[8,64,64]{2,1,0:T(8,128)S(1)} collective-permute-done((f32[8,64,64]{2,1,0:T(8,128)S(1)}, f32[8,64,64]{2,1,0:T(8,128)S(1)}, u32[]{:S(2)}, u32[]{:S(2)}) %collective-permute-start.6) | collective-permute-done | bytes 131104 | tf_op jit(solution)/shard_map/ppermute | solution.py:266
  182.9 3.9 %collective-permute-start.7 = (f32[8,64,64]{2,1,0:T(8,128)S(1)}, f32[8,64,64]{2,1,0:T(8,128)S(1)}, u32[]{:S(2)}, u32[]{:S(2)}) collective-permute-start(f32[8,64,64]{2,1,0:T(8,128)S(1)} %get-tuple-element.29), channel_id=1, source_target_pairs={{0,8},{8,16},{16,24},{1,9},{9,17},{17,25},{2,10},{10,18},{18,26},{... | collective-permute-start | bytes 393224 | tf_op jit(solution)/shard_map/ppermute | solution.py:265
  186.8 1.3 collective-permute-start.8
  188.2 2.5 %collective-permute-done.7 = f32[8,64,64]{2,1,0:T(8,128)S(1)} collective-permute-done((f32[8,64,64]{2,1,0:T(8,128)S(1)}, f32[8,64,64]{2,1,0:T(8,128)S(1)}, u32[]{:S(2)}, u32[]{:S(2)}) %collective-permute-start.7) | collective-permute-done | bytes 131104 | tf_op jit(solution)/shard_map/ppermute | solution.py:265
  190.7 4.4 %collective-permute-done.8 = f32[8,64,64]{2,1,0:T(8,128)S(1)} collective-permute-done((f32[8,64,64]{2,1,0:T(8,128)S(1)}, f32[8,64,64]{2,1,0:T(8,128)S(1)}, u32[]{:S(2)}, u32[]{:S(2)}) %collective-permute-start.8) | collective-permute-done | bytes 131104 | tf_op jit(solution)/shard_map/ppermute | solution.py:266
  196.0 5.0 %merged_norm.1 = bf16[128,512]{1,0:T(8,128)(2,1)} custom-call(f32[2,8,128,128]{3,2,1,0:T(8,128)} %get-tuple-element.7.local_ref, f32[2,8,64,64]{3,2,1,0:T(8,128)} %pad_maximum_fusion.2.state_ref, f32[1,512]{1,0:T(1,128)} %bitcast.193), custom_call_target="tpu_custom_call" | custom-call | flops 251658240 | bytes 2097152 | tf_op jit(solution)/shard_map/merged_norm/pallas_call | solution.py:239
  201.0 3.1 %convolution_add_fusion = f32[128,2048]{1,0:T(8,128)} fusion(bf16[128,512]{1,0:T(8,128)(2,1)} %merged_norm.1, bf16[512,2048]{1,0:T(8,128)(2,1)} %all-gather.5.cloned.1.call-done, f32[128,512]{1,0:T(8,128)S(1)} %get-tuple-element.10, f32[128,512]{1,0:T(8,128)S(1)} %get-tuple-element.11, f32[128,512]{1,0:T(8,128)S(1)} %get-tuple-element.12, ...), kind=kOutput, calls=%fused_computation | convolution fusion | flops 269484032 | bytes 4325376 | tf_op jit(solution)/shard_map/dot_general | solution.py:433
  204.2 6.3 %reduce-scatter.2.cloned.1.call-done = f32[64,2048]{1,0:T(8,128)} async-done(((f32[128,2048]{1,0:T(8,128)}), f32[64,2048]{1,0:T(8,128)}) %reduce-scatter.2.cloned.1.call-update) | async-done | bytes 524304 | tf_op jit(solution)/shard_map/reduce_scatter | solution.py:432
  210.5 1.8 convert_bitcast_fusion
  (128 shorter events, 12.4 us)
Async XLA Ops:
  6.5 79.6 %copy-start = (f32[2,16,64,64]{3,2,1,0:T(8,128)S(1)}, f32[2,16,64,64]{3,2,1,0:T(8,128)}, u32[]{:S(2)}) copy-start(f32[2,16,64,64]{3,2,1,0:T(8,128)} %param.35) | copy-start | bytes 1572868
  6.5 71.3 %all-gather.3.cloned.1.call-start = ((), (), s32[]{:S(2)}) async-start(), calls=%async_computation.3 | async-start | bytes 2949120 | tf_op jit(solution)/shard_map/all_gather | solution.py:343
  12.6 15.6 %copy-start.10 = (bf16[1,128,1024]{2,1,0:T(8,128)(2,1)S(1)}, bf16[1,128,1024]{2,1,0:T(8,128)(2,1)}, u32[]{:S(2)}) copy-start(bf16[1,128,1024]{2,1,0:T(8,128)(2,1)} %param.20) | copy-start | bytes 786436
  27.2 3.5 %copy-start.17 = (f32[2048]{0:T(1024)S(1)}, f32[2048]{0:T(1024)}, u32[]{:S(2)}) copy-start(f32[2048]{0:T(1024)} %param.21) | copy-start | bytes 24580
  28.1 6.4 %copy-start.11 = (bf16[512,128]{1,0:T(8,128)(2,1)S(1)}, bf16[512,128]{1,0:T(8,128)(2,1)}, u32[]{:S(2)}) copy-start(bf16[512,128]{1,0:T(8,128)(2,1)} %param.39) | copy-start | bytes 393220
  28.1 8.7 %copy-start.8 = (bf16[2048,96]{0,1:T(8,128)(2,1)S(1)}, bf16[2048,96]{0,1:T(8,128)(2,1)}, u32[]{:S(2)}) copy-start(bf16[2048,96]{0,1:T(8,128)(2,1)} %param.28) | copy-start | bytes 1179652
  28.1 9.0 %copy-start.9 = (bf16[2048,96]{0,1:T(8,128)(2,1)S(1)}, bf16[2048,96]{0,1:T(8,128)(2,1)}, u32[]{:S(2)}) copy-start(bf16[2048,96]{0,1:T(8,128)(2,1)} %param.32) | copy-start | bytes 1179652
  28.1 172.9 %all-gather.5.cloned.1.call-start = ((), (), s32[]{:S(2)}) async-start(), calls=%async_computation.4 | async-start | bytes 2228224 | tf_op jit(solution)/shard_map/all_gather | solution.py:419
  30.7 6.8 %copy-start.18 = (f32[1,8,128]{2,1,0:T(8,128)S(1)}, f32[1,8,128]{2,1,0:T(8,128)}, u32[]{:S(2)}) copy-start(f32[1,8,128]{2,1,0:T(8,128)} %param.31) | copy-start | bytes 12292
  30.7 8.2 %copy-start.20 = (f32[2,1024]{1,0:T(2,128)S(1)}, f32[2,1024]{1,0:T(2,128)}, u32[]{:S(2)}) copy-start(f32[2,1024]{1,0:T(2,128)} %param.34) | copy-start | bytes 24580
  30.7 8.2 %copy-start.21 = (f32[2,1024]{1,0:T(2,128)S(1)}, f32[2,1024]{1,0:T(2,128)}, u32[]{:S(2)}) copy-start(f32[2,1024]{1,0:T(2,128)} %param.30) | copy-start | bytes 24580
  30.9 15.8 %collective-permute-start.2 = (bf16[128,2048]{1,0:T(8,128)(2,1)S(1)}, bf16[128,2048]{1,0:T(8,128)(2,1)S(1)}, u32[]{:S(2)}, u32[]{:S(2)}) collective-permute-start(bf16[128,2048]{1,0:T(8,128)(2,1)S(1)} %fusion.21), channel_id=1, source_target_pairs={{0,6},{2,4},{4,2},{6,0},{1,7},{3,5},{5,3},{7,1},{8,14},{10,12},{12... | collective-permute-start | bytes 1572872 | tf_op jit(solution)/shard_map/ppermute | solution.py:285
  31.7 26.4 %collective-permute-start.1 = (bf16[128,2048]{1,0:T(8,128)(2,1)S(1)}, bf16[128,2048]{1,0:T(8,128)(2,1)}, u32[]{:S(2)}, u32[]{:S(2)}) collective-permute-start(bf16[128,2048]{1,0:T(8,128)(2,1)S(1)} %fusion.21), channel_id=1, source_target_pairs={{0,4},{2,6},{4,0},{6,2},{1,5},{3,7},{5,1},{7,3},{8,12},{10,14},{12... | collective-permute-start | bytes 1572872 | tf_op jit(solution)/shard_map/ppermute | solution.py:285
  33.2 24.9 %collective-permute-start = (bf16[128,2048]{1,0:T(8,128)(2,1)S(1)}, bf16[128,2048]{1,0:T(8,128)(2,1)}, u32[]{:S(2)}, u32[]{:S(2)}) collective-permute-start(bf16[128,2048]{1,0:T(8,128)(2,1)S(1)} %fusion.21), channel_id=1, source_target_pairs={{0,2},{2,0},{4,6},{6,4},{1,3},{3,1},{5,7},{7,5},{8,10},{10,8},{12,... | collective-permute-start | bytes 1572872 | tf_op jit(solution)/shard_map/ppermute | solution.py:285
  34.5 53.2 %collective-permute-start.13 = (bf16[512,128]{1,0:T(8,128)(2,1)S(1)}, bf16[512,128]{1,0:T(8,128)(2,1)S(1)}, u32[]{:S(2)}, u32[]{:S(2)}) collective-permute-start(bf16[512,128]{1,0:T(8,128)(2,1)S(1)} %copy-done.11), channel_id=1, source_target_pairs={{0,6},{2,4},{4,2},{6,0},{1,7},{3,5},{5,3},{7,1},{8,14},{10,12},{12... | collective-permute-start | bytes 393224 | tf_op jit(solution)/shard_map/ppermute | solution.py:285
  35.2 52.5 %collective-permute-start.12 = (bf16[512,128]{1,0:T(8,128)(2,1)S(1)}, bf16[512,128]{1,0:T(8,128)(2,1)}, u32[]{:S(2)}, u32[]{:S(2)}) collective-permute-start(bf16[512,128]{1,0:T(8,128)(2,1)S(1)} %copy-done.11), channel_id=1, source_target_pairs={{0,4},{2,6},{4,0},{6,2},{1,5},{3,7},{5,1},{7,3},{8,12},{10,14},{12... | collective-permute-start | bytes 393224 | tf_op jit(solution)/shard_map/ppermute | solution.py:285
  38.0 59.4 %copy-start.12 = (f32[128,16]{0,1:T(8,128)}, f32[128,16]{0,1:T(8,128)S(1)}, u32[]{:S(2)}) copy-start(f32[128,16]{0,1:T(8,128)S(1)} %get-tuple-element.57) | copy-start | bytes 24580
  38.0 59.4 %copy-start.14 = (f32[128,16]{0,1:T(8,128)}, f32[128,16]{0,1:T(8,128)S(1)}, u32[]{:S(2)}) copy-start(f32[128,16]{0,1:T(8,128)S(1)} %get-tuple-element.58) | copy-start | bytes 24580
  46.7 41.0 %collective-permute-start.11 = (bf16[512,128]{1,0:T(8,128)(2,1)S(1)}, bf16[512,128]{1,0:T(8,128)(2,1)S(1)}, u32[]{:S(2)}, u32[]{:S(2)}) collective-permute-start(bf16[512,128]{1,0:T(8,128)(2,1)S(1)} %copy-done.11), channel_id=1, source_target_pairs={{0,2},{2,0},{4,6},{6,4},{1,3},{3,1},{5,7},{7,5},{8,10},{10,8},{12,... | collective-permute-start | bytes 393224 | tf_op jit(solution)/shard_map/ppermute | solution.py:285
  82.4 4.0 %copy-start.22 = (f32[1024]{0:T(1024)S(1)}, f32[1024]{0:T(1024)}, u32[]{:S(2)}) copy-start(f32[1024]{0:T(1024)} %param.36) | copy-start | bytes 12292
  82.4 4.6 %copy-start.23 = (f32[16]{0:T(128)S(1)}, f32[16]{0:T(128)}, u32[]{:S(2)}) copy-start(f32[16]{0:T(128)} %param.37) | copy-start | bytes 196
  82.4 13.9 %all-to-all-start.1 = ((bf16[4,128,576]{1,2,0:T(8,128)(2,1)}), bf16[4,128,576]{1,2,0:T(8,128)(2,1)S(1)}, u32[]{:S(2)}, u32[]{:S(2)}) async-start(bf16[4,128,576]{1,2,0:T(8,128)(2,1)} %copy_bitcast_fusion.1), calls=%async_computation.1 | async-start | bytes 1179648 | tf_op jit(solution)/shard_map/all_to_all | solution.py:347
  86.1 124.4 %reduce-scatter.2.cloned.1.call-start = ((), (), s32[]{:S(2)}) async-start(), calls=%async_computation.5 | async-start | bytes 1572864 | tf_op jit(solution)/shard_map/reduce_scatter | solution.py:432
  88.8 2.4 %copy-start.4 = (bf16[512,128]{1,0:T(8,128)(2,1)}, bf16[512,128]{1,0:T(8,128)(2,1)S(1)}, u32[]{:S(2)}) copy-start(bf16[512,128]{1,0:T(8,128)(2,1)S(1)} %get-tuple-element.25) | copy-start | bytes 393220
  88.8 2.3 %copy-start.6 = (bf16[512,128]{1,0:T(8,128)(2,1)}, bf16[512,128]{1,0:T(8,128)(2,1)S(1)}, u32[]{:S(2)}) copy-start(bf16[512,128]{1,0:T(8,128)(2,1)S(1)} %get-tuple-element.26) | copy-start | bytes 393220
  88.8 10.6 %copy-start.2 = (bf16[512,128]{1,0:T(8,128)(2,1)}, bf16[512,128]{1,0:T(8,128)(2,1)S(1)}, u32[]{:S(2)}) copy-start(bf16[512,128]{1,0:T(8,128)(2,1)S(1)} %get-tuple-element.24) | copy-start | bytes 393220
  89.7 74.0 %collective-permute-start.16 = (bf16[512,512]{1,0:T(8,128)(2,1)}, bf16[512,512]{1,0:T(8,128)(2,1)}, u32[]{:S(2)}, u32[]{:S(2)}) collective-permute-start(bf16[512,512]{1,0:T(8,128)(2,1)} %pad_maximum_fusion.4), channel_id=1, source_target_pairs={{0,24},{8,16},{16,8},{24,0},{1,25},{9,17},{17,9},{25,1},{2,26},{10... | collective-permute-start | bytes 1572872 | tf_op jit(solution)/shard_map/ppermute | solution.py:285
  90.9 74.1 %collective-permute-start.15 = (bf16[512,512]{1,0:T(8,128)(2,1)}, bf16[512,512]{1,0:T(8,128)(2,1)}, u32[]{:S(2)}, u32[]{:S(2)}) collective-permute-start(bf16[512,512]{1,0:T(8,128)(2,1)} %pad_maximum_fusion.4), channel_id=1, source_target_pairs={{0,16},{8,24},{16,0},{24,8},{1,17},{9,25},{17,1},{25,9},{2,18},{10... | collective-permute-start | bytes 1572872 | tf_op jit(solution)/shard_map/ppermute | solution.py:285
  91.1 75.6 %collective-permute-start.14 = (bf16[512,512]{1,0:T(8,128)(2,1)}, bf16[512,512]{1,0:T(8,128)(2,1)S(1)}, u32[]{:S(2)}, u32[]{:S(2)}) collective-permute-start(bf16[512,512]{1,0:T(8,128)(2,1)} %pad_maximum_fusion.4), channel_id=1, source_target_pairs={{0,8},{8,0},{16,24},{24,16},{1,9},{9,1},{17,25},{25,17},{2,10},{10... | collective-permute-start | bytes 1572872 | tf_op jit(solution)/shard_map/ppermute | solution.py:285
  98.1 50.7 %collective-permute-start.10 = (bf16[128,256]{0,1:T(8,128)(2,1)}, bf16[128,256]{0,1:T(8,128)(2,1)}, u32[]{:S(2)}, u32[]{:S(2)}) collective-permute-start(bf16[128,256]{0,1:T(8,128)(2,1)} %pad_maximum_fusion.6), channel_id=1, source_target_pairs={{8,0},{16,8},{24,16},{9,1},{17,9},{25,17},{10,2},{18,10},{26,18},{... | collective-permute-start | bytes 196616 | tf_op jit(solution)/shard_map/ppermute | solution.py:28
  99.4 60.6 %collective-permute-start.9 = (bf16[128,256]{0,1:T(8,128)(2,1)}, bf16[128,256]{0,1:T(8,128)(2,1)}, u32[]{:S(2)}, u32[]{:S(2)}) collective-permute-start(bf16[128,256]{0,1:T(8,128)(2,1)} %pad_maximum_fusion.6), channel_id=1, source_target_pairs={{0,8},{8,16},{16,24},{1,9},{9,17},{17,25},{2,10},{10,18},{18,26},{... | collective-permute-start | bytes 196616 | tf_op jit(solution)/shard_map/ppermute | solution.py:25
  146.4 2.4 %copy-start.13 = (f32[128,16]{0,1:T(8,128)S(1)}, f32[128,16]{0,1:T(8,128)}, u32[]{:S(2)}) copy-start(f32[128,16]{0,1:T(8,128)} %copy-done.12) | copy-start | bytes 24580
  146.4 2.4 %copy-start.15 = (f32[128,16]{0,1:T(8,128)S(1)}, f32[128,16]{0,1:T(8,128)}, u32[]{:S(2)}) copy-start(f32[128,16]{0,1:T(8,128)} %copy-done.14) | copy-start | bytes 24580
  148.6 13.8 %copy-start.16 = (pred[128,384]{0,1:T(8,128)(4,1)S(1)}, pred[128,384]{0,1:T(8,128)(4,1)}, u32[]{:S(2)}) copy-start(pred[128,384]{0,1:T(8,128)(4,1)} %fusion.38) | copy-start | bytes 147460
  148.7 14.1 %copy-start.19 = (f32[2,4]{1,0:T(2,128)S(1)}, f32[2,4]{1,0:T(2,128)}, u32[]{:S(2)}) copy-start(f32[2,4]{1,0:T(2,128)} %max.28) | copy-start | bytes 100
  148.8 18.2 %collective-permute-start.3 = (f32[8,64,64]{2,1,0:T(8,128)S(1)}, f32[8,64,64]{2,1,0:T(8,128)S(1)}, u32[]{:S(2)}, u32[]{:S(2)}) collective-permute-start(f32[8,64,64]{2,1,0:T(8,128)S(1)} %get-tuple-element.37), channel_id=1, source_target_pairs={{0,8},{8,16},{16,24},{1,9},{9,17},{17,25},{2,10},{10,18},{18,26},{... | collective-permute-start | bytes 393224 | tf_op jit(solution)/shard_map/ppermute | solution.py:265
  160.0 8.5 %collective-permute-start.4 = (f32[8,64,64]{2,1,0:T(8,128)S(1)}, f32[8,64,64]{2,1,0:T(8,128)S(1)}, u32[]{:S(2)}, u32[]{:S(2)}) collective-permute-start(f32[8,64,64]{2,1,0:T(8,128)S(1)} %get-tuple-element.38), channel_id=1, source_target_pairs={{8,0},{16,8},{24,16},{9,1},{17,9},{25,17},{10,2},{18,10},{26,18},{... | collective-permute-start | bytes 393224 | tf_op jit(solution)/shard_map/ppermute | solution.py:266
  163.7 2.7 %copy-start.3 = (bf16[512,128]{1,0:T(8,128)(2,1)S(1)}, bf16[512,128]{1,0:T(8,128)(2,1)}, u32[]{:S(2)}) copy-start(bf16[512,128]{1,0:T(8,128)(2,1)} %copy-done.2) | copy-start | bytes 393220
  163.7 2.7 %copy-start.5 = (bf16[512,128]{1,0:T(8,128)(2,1)S(1)}, bf16[512,128]{1,0:T(8,128)(2,1)}, u32[]{:S(2)}) copy-start(bf16[512,128]{1,0:T(8,128)(2,1)} %copy-done.4) | copy-start | bytes 393220
  163.7 2.7 %copy-start.7 = (bf16[512,128]{1,0:T(8,128)(2,1)S(1)}, bf16[512,128]{1,0:T(8,128)(2,1)}, u32[]{:S(2)}) copy-start(bf16[512,128]{1,0:T(8,128)(2,1)} %copy-done.6) | copy-start | bytes 393220
  166.7 1.9 copy-start.1
  169.4 8.3 %collective-permute-start.5 = (f32[8,64,64]{2,1,0:T(8,128)S(1)}, f32[8,64,64]{2,1,0:T(8,128)S(1)}, u32[]{:S(2)}, u32[]{:S(2)}) collective-permute-start(f32[8,64,64]{2,1,0:T(8,128)S(1)} %get-tuple-element.33), channel_id=1, source_target_pairs={{0,8},{8,16},{16,24},{1,9},{9,17},{17,25},{2,10},{10,18},{18,26},{... | collective-permute-start | bytes 393224 | tf_op jit(solution)/shard_map/ppermute | solution.py:265
  173.8 8.3 %collective-permute-start.6 = (f32[8,64,64]{2,1,0:T(8,128)S(1)}, f32[8,64,64]{2,1,0:T(8,128)S(1)}, u32[]{:S(2)}, u32[]{:S(2)}) collective-permute-start(f32[8,64,64]{2,1,0:T(8,128)S(1)} %get-tuple-element.34), channel_id=1, source_target_pairs={{8,0},{16,8},{24,16},{9,1},{17,9},{25,17},{10,2},{18,10},{26,18},{... | collective-permute-start | bytes 393224 | tf_op jit(solution)/shard_map/ppermute | solution.py:266
  182.9 7.8 %collective-permute-start.7 = (f32[8,64,64]{2,1,0:T(8,128)S(1)}, f32[8,64,64]{2,1,0:T(8,128)S(1)}, u32[]{:S(2)}, u32[]{:S(2)}) collective-permute-start(f32[8,64,64]{2,1,0:T(8,128)S(1)} %get-tuple-element.29), channel_id=1, source_target_pairs={{0,8},{8,16},{16,24},{1,9},{9,17},{17,25},{2,10},{10,18},{18,26},{... | collective-permute-start | bytes 393224 | tf_op jit(solution)/shard_map/ppermute | solution.py:265
  186.8 8.3 %collective-permute-start.8 = (f32[8,64,64]{2,1,0:T(8,128)S(1)}, f32[8,64,64]{2,1,0:T(8,128)S(1)}, u32[]{:S(2)}, u32[]{:S(2)}) collective-permute-start(f32[8,64,64]{2,1,0:T(8,128)S(1)} %get-tuple-element.30), channel_id=1, source_target_pairs={{8,0},{16,8},{24,16},{9,1},{17,9},{25,17},{10,2},{18,10},{26,18},{... | collective-permute-start | bytes 393224 | tf_op jit(solution)/shard_map/ppermute | solution.py:266
Sparse Core Ops, SparseCore 0:
  28.2 49.5 all-gather.2
  80.6 85.7 all-gather.4
  204.3 6.1 reduce-scatter.1
where the time goes:
time: 220 us; the launch traced here: 219 us
  waiting for transfers between devices  57.5 us (26%)
  Pallas kernels  46.8 us (21%)
  starting transfers between devices  44.7 us (20%)
  matrix products  19.6 us (9%)
  blocking collectives  16.8 us (8%)
  between operations  13.9 us (6%)
  local copies, waits for them, and re-layouts  10.3 us (5%)
  other arithmetic  9.14 us (4%)
    pallas_call x1, Pallas kernels, chunked(): pl.pallas_call(chunk_kernel, grid=(pairs,), in_specs=[role(0), role(1), r...  41.7 us
    all_gather x1, waiting for transfers between devices, local(): whole_cols = lax.all_gather(regrouped, 'sp', axis=0, tiled=True)  19.7 us
    ppermute x3, starting transfers between devices, hop(): forward = lax.ppermute(later[0], 'sp', ups)  19.5 us
    all_to_all x1, blocking collectives, local(): lax.all_to_all(joined, 'fs', split_axis=1, concat_axis=0, tiled=True)  14.5 us
    ppermute x9, waiting for transfers between devices, swapped(): lax.ppermute(block, axis, [(i, i ^ flip) for i in range(count)])  13.9 us
    ppermute x9, starting transfers between devices, swapped(): lax.ppermute(block, axis, [(i, i ^ flip) for i in range(count)])  10.9 us
    ppermute x3, waiting for transfers between devices, hop(): backward = lax.ppermute(later[1], 'sp', downs)  10.4 us
    unnamed x61, local copies, waits for them, and re-layouts  6.35 us
  transfers between devices with their start and end apart: 21, of which 10 were waited for; matrix products, arithmetic and copies ran while one was open for 12% of the time, Pallas kernels for 21%

commit v1 on v0

--- a/solution.py
+++ b/solution.py
@@ -1,5 +1,6 @@
 import jax
 import jax.numpy as jnp
+import numpy as np
 from jax import lax
 from jax.experimental import pallas as pl
 from jax.experimental.pallas import tpu as pltpu
@@ -54,6 +55,7 @@
 CHUNK = 32
 PAIR = 2 * HD
 F32 = jnp.float32
+BF16 = jnp.bfloat16
 NN = (((1,), (0,)), ((), ()))
 NT = (((1,), (1,)), ((), ()))
 
@@ -437,10 +439,1003 @@
     )
     return layer_out.astype(jnp.bfloat16)[None]
 
+MESH_IDS = pl.DeviceIdType.MESH
+
+
+def flipped(index, bits):
+    result = index
+    for bit in (1, 2):
+        if bits & bit:
+            result = result + bit - 2 * bit * lax.rem(lax.div(index, bit), 2)
+    return result
+
+
+def front_kernel(
+    x_ref,
+    wr_ref,
+    wk_ref,
+    wv_ref,
+    wq_ref,
+    kv_ref,
+    extra_ref,
+    dup_ref,
+    eup_ref,
+    gain_ref,
+    ddown_ref,
+    edown_ref,
+    doff_ref,
+    eoff_ref,
+    proj_ref,
+    log_ref,
+    learn_ref,
+    xbuf,
+    wbuf,
+    ebuf,
+    dup,
+    eup,
+    local_sem,
+    wlocal_sem,
+    up_send,
+    up_recv,
+    dn_send,
+    dn_recv,
+    sib_send,
+    sib_recv,
+    wz_send,
+    wz_recv,
+    e_send,
+    e_recv,
+    p_send,
+    p_recv,
+    f_send,
+    f_recv,
+):
+    sp, fs, tp = lax.axis_index("sp"), lax.axis_index("fs"), lax.axis_index("tp")
+    depth = lax.axis_size("sp")
+    width = lax.axis_size("fs")
+    tokens = x_ref.shape[1]
+    rows = wr_ref.shape[0]
+    sibling = {"tp": 1 - tp}
+    plane = ({"fs": flipped(fs, 1)}, {"fs": flipped(fs, 2)})
+
+    def remote(src, dst, send, recv, device):
+        return pltpu.make_async_remote_copy(
+            src_ref=src,
+            dst_ref=dst,
+            send_sem=send,
+            recv_sem=recv,
+            device_id=device,
+            device_id_type=MESH_IDS,
+        )
+
+    def rows_of(z, f):
+        return pl.ds(pl.multiple_of((z * width + f) * rows, rows), rows)
+
+    def pieces(z):
+        low = pl.ds(pl.multiple_of(z * PAIR, PAIR), PAIR)
+        shared = pl.ds(pl.multiple_of(lax.div(z, 2) * PAIR, PAIR), PAIR)
+        return [ref.at[:, low] for ref in (wr_ref, wk_ref, wv_ref, wq_ref)] + [
+            kv_ref.at[:, shared]
+        ]
+
+    def lanes(place):
+        return slice(place * PAIR, (place + 1) * PAIR)
+
+    cols = pl.ds(pl.multiple_of((tp * depth + sp) * PAIR, PAIR), PAIR)
+    own_x = pltpu.make_async_copy(x_ref.at[0], xbuf.at[sp, tp], local_sem.at[0])
+    own_x.start()
+    own_w = [
+        pltpu.make_async_copy(
+            piece, wbuf.at[rows_of(sp, fs), lanes(place)], wlocal_sem.at[place]
+        )
+        for place, piece in enumerate(pieces(sp))
+    ]
+    for copy in own_w:
+        copy.start()
+    small = [
+        pltpu.make_async_copy(extra_ref.at[0], ebuf.at[sp], local_sem.at[1]),
+        pltpu.make_async_copy(dup_ref.at[:, :, cols], dup, local_sem.at[2]),
+        pltpu.make_async_copy(eup_ref.at[:, :, cols], eup, local_sem.at[3]),
+    ]
+    for copy in small:
+        copy.start()
+
+    barrier = pltpu.get_barrier_semaphore()
+    peers = [{"sp": flipped(sp, k)} for k in range(1, depth)] + [sibling, *plane]
+    for peer in peers:
+        pl.semaphore_signal(barrier, inc=1, device_id=peer, device_id_type=MESH_IDS)
+    pl.semaphore_wait(barrier, len(peers))
+
+    def x_move(src_z, send, recv, device, src=None):
+        there = xbuf.at[src_z, tp]
+        return remote(there if src is None else src, there, send, recv, device)
+
+    up_to, dn_to = {"sp": sp + 1}, {"sp": sp - 1}
+
+    @pl.when(sp < depth - 1)
+    def _():
+        x_move(sp, up_send.at[0], up_recv.at[0], up_to, x_ref.at[0]).start()
+
+    @pl.when(sp > 0)
+    def _():
+        x_move(sp, dn_send.at[0], dn_recv.at[0], dn_to, x_ref.at[0]).start()
+
+    def wz_block(k):
+        there = wbuf.at[rows_of(sp, fs)]
+        return remote(there, there, wz_send.at[k - 1], wz_recv.at[k - 1], {"sp": flipped(sp, k)})
+
+    def e_block(k):
+        return remote(
+            extra_ref.at[0],
+            ebuf.at[sp],
+            e_send.at[k - 1],
+            e_recv.at[k - 1],
+            {"sp": flipped(sp, k)},
+        )
+
+    for k in range(1, depth):
+        target = flipped(sp, k)
+        for place, piece in enumerate(pieces(target)):
+            remote(
+                piece,
+                wbuf.at[rows_of(sp, fs), lanes(place)],
+                wz_send.at[k - 1],
+                wz_recv.at[k - 1],
+                {"sp": target},
+            ).start()
+        e_block(k).start()
+
+    own_x.wait()
+    sib = [x_move(sp, sib_send.at[0], sib_recv.at[0], sibling)]
+    sib[0].start()
+    for copy in own_w:
+        copy.wait()
+
+    def p_block(k, side):
+        there = wbuf.at[rows_of(flipped(sp, k), fs)]
+        return remote(there, there, p_send.at[k, side], p_recv.at[k, side], plane[side])
+
+    def f_block(k):
+        side = k % 2
+        there = wbuf.at[rows_of(flipped(sp, k), flipped(fs, 2 if side == 0 else 1))]
+        return remote(there, there, f_send.at[k], f_recv.at[k], plane[side])
+
+    def x_step(k):
+        @pl.when(sp >= k)
+        def _():
+            x_move(sp, up_send.at[k - 1], up_recv.at[k - 1], up_to).wait_recv()
+            if k < depth - 1:
+
+                @pl.when(sp < depth - 1)
+                def _():
+                    x_move(sp - k, up_send.at[k], up_recv.at[k], up_to).start()
+
+            x_move(sp - k, sib_send.at[k], sib_recv.at[k], sibling).start()
+
+        @pl.when(sp < depth - k)
+        def _():
+            x_move(sp, dn_send.at[k - 1], dn_recv.at[k - 1], dn_to).wait_recv()
+            if k < depth - 1:
+
+                @pl.when(sp > 0)
+                def _():
+                    x_move(sp + k, dn_send.at[k], dn_recv.at[k], dn_to).start()
+
+            x_move(sp + k, sib_send.at[depth + k - 1], sib_recv.at[depth + k - 1], sibling).start()
+
+    def w_step(k):
+        wz_block(k).wait_recv()
+        for side in range(2):
+            p_block(k, side).start()
+
+    def f_step(k):
+        for side in range(2):
+            p_block(k, side).wait_recv()
+        f_block(k).start()
+
+    for side in range(2):
+        p_block(0, side).start()
+    f_step(0)
+    x_step(1)
+    w_step(1)
+    w_step(2)
+    f_step(1)
+    x_step(2)
+    w_step(3)
+    f_step(2)
+    f_step(3)
+    x_step(3)
+    for k in range(depth):
+        f_block(k).wait_recv()
+    for k in range(1, depth):
+        e_block(k).wait_recv()
+    x_move(sp, sib_send.at[0], sib_recv.at[0], sibling).wait_recv()
+    for k in range(1, depth):
+
+        @pl.when(sp >= k)
+        def _():
+            x_move(sp, sib_send.at[k], sib_recv.at[k], sibling).wait_recv()
+
+        @pl.when(sp < depth - k)
+        def _():
+            place = depth + k - 1
+            x_move(sp, sib_send.at[place], sib_recv.at[place], sibling).wait_recv()
+
+    for copy in small:
+        copy.wait()
+
+    gain = gain_ref[...]
+    half = gain.shape[1] // 2
+    doff = doff_ref[:, cols]
+    eoff = eoff_ref[:, cols]
+
+    def block(z, carry):
+        parts = [xbuf[z, side].astype(F32) for side in range(2)]
+        total = sum(jnp.sum(part * part, axis=1, keepdims=True) for part in parts)
+        scale = lax.rsqrt(total / (2 * half) + NORM_EPS)
+        hidden = jnp.concatenate(
+            [
+                (part * scale * gain[:, side * half : (side + 1) * half]).astype(BF16)
+                for side, part in enumerate(parts)
+            ],
+            axis=1,
+        )
+        where = pl.ds(pl.multiple_of(z * tokens, tokens), tokens)
+
+        def dot(left, right):
+            return jnp.dot(left, right, preferred_element_type=F32)
+
+        proj_ref[where, :] = dot(hidden, wbuf[...]).astype(BF16)
+        decay_act = jnp.tanh(dot(hidden, ddown_ref[...]).astype(BF16).astype(F32)).astype(BF16)
+        learn_low = dot(hidden, edown_ref[...]).astype(BF16)
+        first_head = 2 * sp
+        spikes = jnp.concatenate(
+            [
+                jnp.broadcast_to(ebuf[z, pl.ds(first_head + head, 1), :], (HD, tokens))
+                for head in range(2)
+            ],
+            axis=0,
+        ).T
+        for direction in range(2):
+            pre = doff[direction : direction + 1] + dot(decay_act, dup[direction])
+            softplus = jnp.maximum(-pre, 0.0) + jnp.log1p(jnp.exp(-jnp.abs(pre)))
+            log_ref[direction, where, :] = spikes - jnp.exp(-softplus - 0.5)
+            learn = eoff[direction : direction + 1] + dot(learn_low, eup[direction])
+            learn_ref[direction, where, :] = jax.nn.sigmoid(learn)
+        return carry
+
+    lax.fori_loop(0, depth, block, 0)
+
+    @pl.when(sp < depth - 1)
+    def _():
+        x_move(sp, up_send.at[0], up_recv.at[0], up_to, x_ref.at[0]).wait_send()
+
+    @pl.when(sp > 0)
+    def _():
+        x_move(sp, dn_send.at[0], dn_recv.at[0], dn_to, x_ref.at[0]).wait_send()
+
+    x_move(sp, sib_send.at[0], sib_recv.at[0], sibling).wait_send()
+    for k in range(1, depth):
+
+        @pl.when(sp >= k)
+        def _():
+            x_move(sp, sib_send.at[k], sib_recv.at[k], sibling).wait_send()
+            if k < depth - 1:
+
+                @pl.when(sp < depth - 1)
+                def _():
+                    x_move(sp, up_send.at[k], up_recv.at[k], up_to).wait_send()
+
+        @pl.when(sp < depth - k)
+        def _():
+            place = depth + k - 1
+            x_move(sp, sib_send.at[place], sib_recv.at[place], sibling).wait_send()
+            if k < depth - 1:
+
+                @pl.when(sp > 0)
+                def _():
+                    x_move(sp, dn_send.at[k], dn_recv.at[k], dn_to).wait_send()
+
+        wz_block(k).wait_send()
+        e_block(k).wait_send()
+    for k in range(depth):
+        for side in range(2):
+            p_block(k, side).wait_send()
+        f_block(k).wait_send()
+
+
+def front(inputs, gain, weights, kv, extra, ddown, dup, doff, edown, eup, eoff):
+    depth = lax.axis_size("sp")
+    width = lax.axis_size("fs")
+    _, tokens, half = inputs.shape
+    total = tokens * depth
+    dma = pltpu.SemaphoreType.DMA
+    any_spec = pl.BlockSpec(memory_space=pl.ANY)
+    vmem_spec = pl.BlockSpec(memory_space=pltpu.VMEM)
+    low = ddown.shape[1]
+    return pl.pallas_call(
+        front_kernel,
+        in_specs=[any_spec] * 9 + [vmem_spec] * 5,
+        out_specs=[vmem_spec] * 3,
+        out_shape=[
+            jax.ShapeDtypeStruct((total, 5 * PAIR), BF16),
+            jax.ShapeDtypeStruct((2, total, PAIR), F32),
+            jax.ShapeDtypeStruct((2, total, PAIR), F32),
+        ],
+        scratch_shapes=[
+            pltpu.VMEM((depth, 2, tokens, half), BF16),
+            pltpu.VMEM((2 * half, 5 * PAIR), BF16),
+            pltpu.VMEM((depth, extra.shape[1], tokens), F32),
+            pltpu.VMEM((2, low, PAIR), BF16),
+            pltpu.VMEM((2, low, PAIR), BF16),
+            dma((4,)),
+            dma((5,)),
+            dma((depth,)),
+            dma((depth,)),
+            dma((depth,)),
+            dma((depth,)),
+            dma((2 * depth,)),
+            dma((2 * depth,)),
+            dma((depth - 1,)),
+            dma((depth - 1,)),
+            dma((depth - 1,)),
+            dma((depth - 1,)),
+            dma((width, 2)),
+            dma((width, 2)),
+            dma((width,)),
+            dma((width,)),
+        ],
+        compiler_params=pltpu.CompilerParams(collective_id=0, has_side_effects=True),
+        name="front",
+    )(
+        inputs,
+        *weights,
+        kv,
+        extra,
+        dup,
+        eup,
+        gain[None, :],
+        ddown,
+        edown,
+        doff,
+        eoff,
+    )
+
+
+SPAN = HD
+BATCH = 4
+QUAD = 4 * HD
+TN = (((0,), (0,)), ((), ()))
+
+
+def mm(left, right, dims=NN):
+    return lax.dot_general(left, right, dims, preferred_element_type=F32)
+
+
+def rope_tables(total):
+    quarter = HD // 4
+    inverse = ROPE_BASE ** (-np.arange(quarter, dtype=np.float32) / np.float32(quarter))
+    inverse = inverse.astype(np.float32)
+    lane = np.arange(PAIR) % HD
+    rates = inverse[lane % quarter]
+    sign = np.where(lane % (2 * quarter) < quarter, -1.0, 1.0)
+    coords = np.concatenate([np.arange(total // GRID_W), np.arange(GRID_W)])
+    angles = (coords.astype(np.float32)[:, None] * rates[None, :]).astype(np.float64)
+    return np.stack([np.cos(angles), np.sin(angles) * sign]).astype(np.float32)
+
+
+def mix_body(
+    hook, proj_ref, log_ref, learn_ref, table_ref, gain, sinks, states, mix_ref, s_w, s_read, s_m, s_a, s_local, s_re, s_lin, kpad, vpad, s_q
+):
+    total = proj_ref.shape[0]
+    count = total // SPAN
+    lane = lax.broadcasted_iota(jnp.int32, (SPAN, PAIR), 1)
+    first = lane < HD
+    ones = (
+        jnp.where(first, 1.0, 0.0).astype(BF16),
+        jnp.where(first, 0.0, 1.0).astype(BF16),
+    )
+    nothing = jnp.zeros((SPAN, PAIR), BF16)
+    quad_row = lax.broadcasted_iota(jnp.int32, (SPAN, QUAD), 0)
+    quad_lane = lax.broadcasted_iota(jnp.int32, (SPAN, QUAD), 1)
+    quad_col = lax.rem(quad_lane, HD)
+    ahead = quad_lane < PAIR
+    before = jnp.where(ahead, quad_col - quad_row, quad_row - quad_col)
+    strict, upto = before < 0, before <= 0
+    eye = jnp.where(before == 0, 1.0, 0.0)
+
+    def level(size):
+        return (lax.div(quad_row, 2 * size) == lax.div(quad_col, 2 * size)) & (
+            lax.div(quad_row, size) != lax.div(quad_col, size)
+        )
+
+    square_i = lax.broadcasted_iota(jnp.int32, (QUAD, QUAD), 0)
+    square_j = lax.broadcasted_iota(jnp.int32, (QUAD, QUAD), 1)
+    same_unit = lax.div(square_i, HD) == lax.div(square_j, HD)
+    square_eye = square_i == square_j
+    tri_i = lax.broadcasted_iota(jnp.int32, (SPAN, SPAN), 0)
+    tri_j = lax.broadcasted_iota(jnp.int32, (SPAN, SPAN), 1)
+    tri = [
+        jnp.where(tri_j <= tri_i, 1.0, 0.0).astype(BF16),
+        jnp.where(tri_j >= tri_i, 1.0, 0.0).astype(BF16),
+    ]
+    tri = [jnp.concatenate([one] * 3, axis=1) for one in tri]
+
+    def diagonal(quad):
+        left, right = quad[:, :PAIR], quad[:, PAIR:]
+        return jnp.concatenate(
+            [jnp.concatenate([left * one, nothing], axis=1) for one in ones]
+            + [jnp.concatenate([nothing, right * one], axis=1) for one in ones],
+            axis=0,
+        )
+
+    def quad_dot(lefts, right, dims=NN):
+        highs, lows = zip(*[halves(left) for left in lefts])
+        right_high, right_low = halves(right)
+        count_left = len(lefts)
+        outer = mm(jnp.concatenate(highs + lows, axis=0), diagonal(right_high), dims)
+        inner = mm(jnp.concatenate(highs, axis=0), diagonal(right_low), dims)
+        return [
+            outer[k * SPAN : (k + 1) * SPAN]
+            + (
+                outer[(count_left + k) * SPAN : (count_left + k + 1) * SPAN]
+                + inner[k * SPAN : (k + 1) * SPAN]
+            )
+            for k in range(count_left)
+        ]
+
+    def single(left, right):
+        return mm(left.astype(BF16), diagonal(right.astype(BF16)))
+
+    def rows_at(place):
+        return pl.ds(pl.multiple_of(place * SPAN, SPAN), SPAN)
+
+    def head_sum(value):
+        low = jnp.sum(jnp.where(first, value, 0.0), axis=1, keepdims=True)
+        high = jnp.sum(jnp.where(first, 0.0, value), axis=1, keepdims=True)
+        return jnp.where(first, low, high)
+
+    def prepare(direction, rows):
+        read = proj_ref[rows, :PAIR].astype(F32)
+        key = proj_ref[rows, PAIR : 2 * PAIR].astype(F32)
+        log_decay = log_ref[direction, rows, :]
+        unit = key * lax.rsqrt(head_sum(key * key) + NORM_EPS)
+        erase = unit * learn_ref[direction, rows, :]
+        high = log_decay.astype(BF16)
+        rest = log_decay - high.astype(F32)
+        middle_part = rest.astype(BF16)
+        low = (rest - middle_part.astype(F32)).astype(BF16)
+        total_log = mm(tri[direction], jnp.concatenate([high, middle_part, low], axis=0))
+        end = SPAN - 1 if direction == 0 else 0
+        span_log = total_log[end : end + 1, :]
+        middle = 0.5 * span_log
+        prior_log = total_log - log_decay
+        inverse = jnp.exp(middle - total_log)
+        left = jnp.exp(span_log - total_log)
+        readers = jnp.concatenate(
+            [jnp.exp(prior_log - middle) * unit, jnp.exp(total_log - middle) * read], axis=0
+        )
+        sources = jnp.concatenate([erase * inverse, key * inverse], axis=0)
+        high_r, low_r = halves(readers)
+        high_s, low_s = halves(sources)
+
+        def spread(value):
+            top, bottom = value[:SPAN], value[SPAN:]
+            return jnp.concatenate([top * one for one in ones] + [bottom * one for one in ones], axis=0)
+
+        high_s, low_s = spread(high_s), spread(low_s)
+        meets = mm(
+            jnp.concatenate([high_r, low_r, high_r], axis=1),
+            jnp.concatenate([high_s, high_s, low_s], axis=1),
+            NT,
+        )
+        return (
+            meets,
+            jnp.exp(prior_log) * unit,
+            jnp.exp(total_log) * read,
+            key * left,
+            erase * left,
+            jnp.exp(span_log),
+        )
+
+    def both(one, other):
+        return jnp.concatenate([one, other], axis=1)
+
+    def batch(index, carry, size):
+        groups = [index * size + k for k in range(size)]
+        erased, seens, read_eraseds, starts, lefts, finals, spans, values = [], [], [], [], [], [], [], []
+        for group in groups:
+            rows = (rows_at(group), rows_at(count - 1 - group))
+            parts = [prepare(direction, rows[direction]) for direction in range(2)]
+            meets = [part[0] for part in parts]
+            value = both(*[proj_ref[row, 2 * PAIR : 3 * PAIR] for row in rows])
+            erased.append(
+                jnp.where(strict, both(meets[0][:SPAN, :PAIR], meets[1][:SPAN, :PAIR]), 0.0)
+            )
+            seen = jnp.where(strict, both(meets[0][:SPAN, PAIR:], meets[1][:SPAN, PAIR:]), 0.0)
+            s_re[group] = jnp.where(
+                upto, both(meets[0][SPAN:, :PAIR], meets[1][SPAN:, :PAIR]), 0.0
+            )
+            read_seen = jnp.where(upto, both(meets[0][SPAN:, PAIR:], meets[1][SPAN:, PAIR:]), 0.0)
+            starts.append(both(parts[0][1], parts[1][1]))
+            s_read[group] = both(parts[0][2], parts[1][2])
+            lefts.append((both(parts[0][3], parts[1][3]), both(parts[0][4], parts[1][4])))
+            spans.append(both(parts[0][5], parts[1][5]))
+            values.append(value)
+            pieces = jnp.concatenate([*halves(seen), *halves(read_seen)], axis=0)
+            met = mm(pieces, diagonal(value))
+            seens.append(met[:SPAN] + met[SPAN : 2 * SPAN])
+            s_local[group] = met[2 * SPAN : 3 * SPAN] + met[3 * SPAN :]
+        solves = [eye - jnp.where(level(1), one, 0.0) for one in erased]
+        width = 2
+        while width < SPAN:
+            at = level(width)
+            firsts = [single(solve, jnp.where(at, one, 0.0)) for solve, one in zip(solves, erased)]
+            solves = [solve - single(one, solve) for solve, one in zip(solves, firsts)]
+            width *= 2
+        misses = [
+            eye - solve - quad_dot([one], solve)[0] for solve, one in zip(solves, erased)
+        ]
+        solves = [solve + single(solve, miss) for solve, miss in zip(solves, misses)]
+        maps = [quad_dot([solve], start)[0] for solve, start in zip(solves, starts)]
+        shifts = [quad_dot([solve], seen)[0] for solve, seen in zip(solves, seens)]
+        for place, group in enumerate(groups):
+            key_left, erase_left = lefts[place]
+            s_w[group] = jnp.concatenate([maps[place], shifts[place]], axis=1)
+            map_high, map_low = halves(maps[place])
+            left_high, left_low = halves(erase_left)
+            fade = mm(
+                jnp.concatenate([map_high, map_low, map_high], axis=0),
+                jnp.concatenate([left_high, left_high, left_low], axis=0),
+                TN,
+            )
+            s_m[group] = jnp.where(square_eye, spans[place], 0.0) - jnp.where(same_unit, fade, 0.0)
+            shift_high, shift_low = halves(shifts[place])
+            key_high, key_low = halves(key_left)
+            gained = mm(
+                jnp.concatenate(
+                    [values[place], values[place], shift_high, shift_low, shift_high], axis=0
+                ),
+                jnp.concatenate(
+                    [key_high, key_low, -left_high, -left_high, -left_low], axis=0
+                ),
+                TN,
+            )
+            gained = jnp.where(same_unit, gained, 0.0)
+            s_a[group] = (gained[:SPAN] + gained[SPAN : 2 * SPAN]) + (
+                gained[2 * SPAN : 3 * SPAN] + gained[3 * SPAN :]
+            )
+        return carry
+
+    size = min(BATCH, count)
+    for index in range(count // size):
+        batch(index, 0, size)
+        hook()
+
+    def advance(group, state):
+        high, low = halves(state)
+        step_high, step_low = halves(s_m[group])
+        outer = mm(jnp.concatenate([high, low], axis=0), step_high)
+        inner = mm(high, step_low)
+        following = outer[:SPAN] + (outer[SPAN:] + inner) + s_a[group]
+        s_a[group] = state
+        return following
+
+    state = states
+    for group in range(count):
+        state = advance(group, state)
+    hook()
+
+    def finish(group, carry):
+        maps, shift = s_w[group, :, :QUAD], s_w[group, :, QUAD:]
+        dropped, seen_state = quad_dot([maps, s_read[group]], s_a[group], NT)
+        dropped = dropped + shift
+        out = seen_state + s_local[group] - quad_dot([s_re[group]], dropped)[0]
+        s_lin[0, rows_at(group), :] = out[:, :PAIR]
+        s_lin[1, rows_at(count - 1 - group), :] = out[:, PAIR:]
+        return carry
+
+    def finish_batch(index, carry):
+        for k in range(size):
+            carry = finish(index * size + k, carry)
+        return carry
+
+    lax.fori_loop(0, count // size, finish_batch, 0)
+    hook()
+
+    quarter = HD // 4
+    back = lax.rem(lane, 2 * quarter) >= quarter
+    by_row = lax.rem(lane, HD) < 2 * quarter
+    grid = total // GRID_W
+    edge = jnp.zeros((WINDOW, PAIR), BF16)
+    for ref in (kpad, vpad):
+        ref[:WINDOW, :] = edge
+        ref[WINDOW + total :, :] = edge
+
+    def turned(value, cosine, sine):
+        partner = jnp.where(
+            back, pltpu.roll(value, quarter, 1), pltpu.roll(value, PAIR - quarter, 1)
+        )
+        return value * cosine + partner * sine
+
+    def turn(place, carry):
+        rows = rows_at(place)
+        cosine, sine = [
+            jnp.where(
+                by_row,
+                table_ref[which, pl.ds(place, 1), :],
+                table_ref[which, grid : grid + GRID_W, :],
+            )
+            for which in range(2)
+        ]
+        query = proj_ref[rows, 3 * PAIR : 4 * PAIR].astype(F32)
+        pair = proj_ref[rows, 4 * PAIR :].astype(F32)
+        s_q[rows, :] = turned(query, cosine, sine).astype(BF16)
+        key = jnp.where(first, turned(pair, cosine, sine), 0.0)
+        value = jnp.where(first, 0.0, pair)
+        there = pl.ds(pl.multiple_of(WINDOW + place * SPAN, SPAN), SPAN)
+        kpad[there, :] = (key + pltpu.roll(key, HD, 1)).astype(BF16)
+        vpad[there, :] = (value + pltpu.roll(value, HD, 1)).astype(BF16)
+        return carry
+
+    lax.fori_loop(0, grid, turn, 0)
+    reach = ATT_BLOCK + 2 * WINDOW
+    ahead_of = lax.broadcasted_iota(jnp.int32, (ATT_BLOCK, reach), 1) - (
+        WINDOW + lax.broadcasted_iota(jnp.int32, (ATT_BLOCK, reach), 0)
+    )
+    near = jnp.abs(ahead_of) <= WINDOW
+    key_at = lax.broadcasted_iota(jnp.int32, (ATT_BLOCK, reach), 1) - WINDOW
+    mine = lax.broadcasted_iota(jnp.int32, (ATT_BLOCK, PAIR), 1) < HD
+
+    def attend(place, carry):
+        start = pl.multiple_of(place * ATT_BLOCK, ATT_BLOCK)
+        rows = pl.ds(start, ATT_BLOCK)
+        query = s_q[rows, :]
+        keys = kpad[pl.ds(start, reach), :]
+        held = vpad[pl.ds(start, reach), :]
+        allowed = near & (key_at >= -start) & (key_at < total - start)
+        mixed = []
+        for head in range(2):
+            own = jnp.where(mine if head == 0 else jnp.logical_not(mine), query.astype(F32), 0.0)
+            scores = mm(own.astype(BF16), keys, NT) * HD ** (-0.5)
+            scores = jnp.where(allowed, scores, -jnp.inf)
+            top = jnp.maximum(jnp.max(scores, axis=1, keepdims=True), sinks[head])
+            raised = jnp.exp(scores - top)
+            bottom = jnp.exp(sinks[head] - top) + jnp.sum(raised, axis=1, keepdims=True)
+            mixed.append(mm((raised / bottom).astype(BF16), held))
+        mix_ref[rows, PAIR:] = jnp.where(mine, mixed[0], mixed[1]).astype(BF16)
+        return carry
+
+    lax.fori_loop(0, total // ATT_BLOCK, attend, 0)
+    hook()
+
+    def norm(place, carry):
+        rows = rows_at(place)
+        lin_sum = s_lin[0, rows, :] + s_lin[1, rows, :]
+        centred = lin_sum - head_sum(lin_sum) * (1.0 / HD)
+        spread = head_sum(centred * centred) * (1.0 / HD)
+        mix_ref[rows, :PAIR] = (centred * lax.rsqrt(spread + GROUP_EPS) * gain).astype(BF16)
+        return carry
+
+    lax.fori_loop(0, count, norm, 0)
+
+
+def mix_scratch(total):
+    count = total // SPAN
+    return [
+        pltpu.VMEM((count, SPAN, 2 * QUAD), F32),
+        pltpu.VMEM((count, SPAN, QUAD), F32),
+        pltpu.VMEM((count, QUAD, QUAD), F32),
+        pltpu.VMEM((count, SPAN, QUAD), F32),
+        pltpu.VMEM((count, SPAN, QUAD), F32),
+        pltpu.VMEM((count, SPAN, QUAD), F32),
+        pltpu.VMEM((2, total, PAIR), F32),
+        pltpu.VMEM((total + 2 * WINDOW, PAIR), BF16),
+        pltpu.VMEM((total + 2 * WINDOW, PAIR), BF16),
+        pltpu.VMEM((total, PAIR), BF16),
+    ]
+
+
+def back_kernel(
+    lin_ref,
+    win_ref,
+    init_ref,
+    sink_ref,
+    proj_ref,
+    log_ref,
+    learn_ref,
+    table_ref,
+    gain_ref,
+    out_ref,
+    owb,
+    mbuf,
+    mix_ref,
+    init,
+    local_sem,
+    z_send,
+    z_recv,
+    p_send,
+    p_recv,
+    f_send,
+    f_recv,
+    sib_send,
+    sib_recv,
+    m_send,
+    m_recv,
+    *scratch,
+):
+    sp, fs, tp = lax.axis_index("sp"), lax.axis_index("fs"), lax.axis_index("tp")
+    depth = lax.axis_size("sp")
+    width = lax.axis_size("fs")
+    sides = lax.axis_size("tp")
+    rows, cols = lin_ref.shape
+    share = out_ref.shape[1]
+    sibling = {"tp": 1 - tp}
+    plane = ({"fs": flipped(fs, 1)}, {"fs": flipped(fs, 2)})
+
+    def remote(src, dst, send, recv, device):
+        return pltpu.make_async_remote_copy(
+            src_ref=src,
+            dst_ref=dst,
+            send_sem=send,
+            recv_sem=recv,
+            device_id=device,
+            device_id_type=MESH_IDS,
+        )
+
+    def cols_of(z, f, many=1):
+        return pl.ds(pl.multiple_of((z * width + f) * cols, cols), many * cols)
+
+    local = [
+        pltpu.make_async_copy(
+            ref, owb.at[tp, pl.ds(place * rows, rows), cols_of(sp, fs)], local_sem.at[place]
+        )
+        for place, ref in enumerate((lin_ref, win_ref))
+    ]
+    head = (tp * depth + sp) * 2
+    local.append(pltpu.make_async_copy(init_ref.at[:, pl.ds(head, 2)], init, local_sem.at[2]))
+    for copy in local:
+        copy.start()
+    barrier = pltpu.get_barrier_semaphore()
+    pairs = [(k, t) for k in range(depth) for t in range(sides) if k or t]
+    peers = [{"sp": flipped(sp, k), "tp": tp + t - 2 * t * tp} for k, t in pairs] + [*plane]
+    for peer in peers:
+        pl.semaphore_signal(barrier, inc=1, device_id=peer, device_id_type=MESH_IDS)
+    pl.semaphore_wait(barrier, len(peers))
+    for copy in local:
+        copy.wait()
+
+    def z_block(k):
+        there = owb.at[tp, :, cols_of(sp, fs)]
+        return remote(there, there, z_send.at[k - 1], z_recv.at[k - 1], {"sp": flipped(sp, k)})
+
+    def p_block(k, side):
+        there = owb.at[tp, :, cols_of(flipped(sp, k), fs)]
+        return remote(there, there, p_send.at[k, side], p_recv.at[k, side], plane[side])
+
+    def f_block(k):
+        side = k % 2
+        there = owb.at[tp, :, cols_of(flipped(sp, k), flipped(fs, 2 if side == 0 else 1))]
+        return remote(there, there, f_send.at[k], f_recv.at[k], plane[side])
+
+    def s_block(k):
+        there = owb.at[tp, :, cols_of(flipped(sp, k), 0, width)]
+        return remote(there, there, sib_send.at[k], sib_recv.at[k], sibling)
+
+    def w_step(k):
+        if k:
+            z_block(k).wait_recv()
+        for side in range(2):
+            p_block(k, side).start()
+
+    def f_step(k):
+        for side in range(2):
+            p_block(k, side).wait_recv()
+        f_block(k).start()
+
+    def s_step(k):
+        f_block(k).wait_recv()
+        s_block(k).start()
+
+    for k in range(1, depth):
+        z_block(k).start()
+    w_step(0)
+    plan = [
+        [(f_step, 0), (w_step, 1)],
+        [(s_step, 0), (w_step, 2)],
+        [(f_step, 1)],
+        [(w_step, 3), (s_step, 1)],
+        [(f_step, 2)],
+    ]
+    queue = iter(plan)
+
+    def hook():
+        for step, k in next(queue, ()):
+            step(k)
+
+    states = jnp.concatenate([init[d, h] for d in range(2) for h in range(2)], axis=1)
+    lanes = pl.ds(pl.multiple_of((tp * depth + sp) * PAIR, PAIR), PAIR)
+    mix_body(
+        hook,
+        proj_ref,
+        log_ref,
+        learn_ref,
+        table_ref,
+        gain_ref[:, lanes],
+        [sink_ref[0, head], sink_ref[0, head + 1]],
+        states,
+        mix_ref,
+        *scratch,
+    )
+
+    def m_block(k, t):
+        z, side = flipped(sp, k), tp + t - 2 * t * tp
+        start = pl.multiple_of((z * sides + side) * share, share)
+        return remote(
+            mix_ref.at[pl.ds(start, share)],
+            mbuf.at[sp * sides + tp],
+            m_send.at[k * sides + t],
+            m_recv.at[k * sides + t],
+            {"sp": z, "tp": side},
+        )
+
+    for k, t in pairs:
+        m_block(k, t).start()
+    mine = sp * sides + tp
+    mbuf[mine] = mix_ref[pl.ds(pl.multiple_of(mine * share, share), share), :]
+    f_step(3)
+    s_step(2)
+    s_step(3)
+    for k, t in pairs:
+        m_block(k, t).wait_recv()
+    lefts = [
+        jnp.concatenate(
+            [mbuf[z * sides + side, :, :PAIR] for z in range(depth)]
+            + [mbuf[z * sides + side, :, PAIR:] for z in range(depth)],
+            axis=1,
+        )
+        for side in range(sides)
+    ]
+    for k in range(depth):
+        s_block(k).wait_recv()
+        span = cols_of(flipped(sp, k), 0, width)
+        out_ref[0, :, span] = sum(
+            jnp.dot(lefts[side], owb[side, :, span], preferred_element_type=F32)
+            for side in range(sides)
+        ).astype(BF16)
+    for k in range(depth):
+        if k:
+            z_block(k).wait_send()
+        for side in range(2):
+            p_block(k, side).wait_send()
+        f_block(k).wait_send()
+        s_block(k).wait_send()
+    for k, t in pairs:
+        m_block(k, t).wait_send()
+
+
+def back(proj, logs, learn, gain, sink, init, lin_weight, win_weight):
+    depth = lax.axis_size("sp")
+    width = lax.axis_size("fs")
+    sides = lax.axis_size("tp")
+    total = proj.shape[0]
+    rows, cols = lin_weight.shape
+    share = total // (depth * sides)
+    dma = pltpu.SemaphoreType.DMA
+    any_spec = pl.BlockSpec(memory_space=pl.ANY)
+    vmem_spec = pl.BlockSpec(memory_space=pltpu.VMEM)
+    features = cols * depth * width
+    return pl.pallas_call(
+        back_kernel,
+        in_specs=[any_spec] * 3 + [pl.BlockSpec(memory_space=pltpu.SMEM)] + [vmem_spec] * 5,
+        out_specs=vmem_spec,
+        out_shape=jax.ShapeDtypeStruct((1, share, features), BF16),
+        scratch_shapes=[
+            pltpu.VMEM((sides, 2 * rows, features), BF16),
+            pltpu.VMEM((depth * sides, share, 2 * PAIR), BF16),
+            pltpu.VMEM((total, 2 * PAIR), BF16),
+            pltpu.VMEM((2, 2, HD, HD), F32),
+            dma((3,)),
+            dma((depth - 1,)),
+            dma((depth - 1,)),
+            dma((depth, 2)),
+            dma((depth, 2)),
+            dma((depth,)),
+            dma((depth,)),
+            dma((depth,)),
+            dma((depth,)),
+            dma((depth * sides,)),
+            dma((depth * sides,)),
+        ]
+        + mix_scratch(total),
+        compiler_params=pltpu.CompilerParams(
+            collective_id=1, has_side_effects=True, vmem_limit_bytes=60 * 2**20
+        ),
+        name="back",
+    )(
+        lin_weight,
+        win_weight,
+        init,
+        sink[None, :],
+        proj,
+        logs,
+        learn,
+        jnp.asarray(rope_tables(total)),
+        gain[None, :],
+    )
+
+
+def by_heads(
+    inputs,
+    input_norm_gain,
+    receptance_weight,
+    linear_key_weight,
+    linear_value_weight,
+    window_query_weight,
+    window_key_weight,
+    window_value_weight,
+    decay_down_weight,
+    decay_up_weight,
+    decay_offset,
+    decay_log_extra,
+    erasure_down_weight,
+    erasure_up_weight,
+    erasure_offset,
+    initial_state,
+    head_norm_gain,
+    query_sink_logit,
+    linear_output_weight,
+    window_output_weight,
+):
+    count = window_key_weight.shape[0]
+    kv = jnp.concatenate(
+        [
+            weight.reshape(count, -1, HD)
+            for weight in (window_key_weight, window_value_weight)
+        ],
+        axis=2,
+    ).reshape(count, -1)
+    proj, logs, learn = front(
+        inputs,
+        input_norm_gain,
+        (receptance_weight, linear_key_weight, linear_value_weight, window_query_weight),
+        kv,
+        decay_log_extra,
+        decay_down_weight,
+        decay_up_weight,
+        decay_offset,
+        erasure_down_weight,
+        erasure_up_weight,
+        erasure_offset,
+    )
+    return back(
+        proj,
+        logs,
+        learn,
+        head_norm_gain,
+        query_sink_logit,
+        initial_state,
+        linear_output_weight,
+        window_output_weight,
+    )
+
+
+def layer(*arrays):
+    inputs, recept, keys = arrays[0], arrays[2], arrays[6]
+    depth, width, sides = [lax.axis_size(axis) for axis in ("sp", "fs", "tp")]
+    fits = (
+        recept.shape[1] == arrays[5].shape[1] == depth * PAIR
+        and 2 * keys.shape[1] == depth * HD
+        and (depth, width, sides) == (4, 4, 2)
+        and inputs.shape[1] % WINDOW == 0
+        and SPAN == GRID_W
+    )
+    return (by_heads if fits else local)(*arrays)
+
 
 def solution(mesh):
     return jax.shard_map(
-        local,
+        layer,
         mesh=mesh,
         in_specs=(
             P("fs", "sp", "tp"),

time: 220 us -> 109 us (0.50)
  waiting for transfers between devices: 57.5 us -> 0 us
  Pallas kernels: 46.8 us -> 102 us
  starting transfers between devices: 44.7 us -> 0 us
  matrix products: 19.6 us -> 0 us
  blocking collectives: 16.8 us -> 0 us
  between operations: 13.9 us -> 0.04 us
  other arithmetic: 9.14 us -> 0.01 us
  local copies, waits for them, and re-layouts: 10.3 us -> 6.23 us
    pallas_call x2, Pallas kernels: 46.8 us -> 102 us  [the longest x1 54.9 us: back(): pl.pallas_call(back_kernel, in_specs=[any_spec] * 3 + [pl.BlockSpec(memor...]
    ppermute x17 -> x0, starting transfers between devices: 41 us -> none  [the longest x3 19.5 us: hop(): forward = lax.ppermute(later[0], 'sp', ups)]
    ppermute x17 -> x0, waiting for transfers between devices: 29.2 us -> none  [the longest x9 13.9 us: swapped(): lax.ppermute(block, axis, [(i, i ^ flip) for i in range(count)])]
    all_gather x2 -> x0, waiting for transfers between devices: 19.7 us -> none  [the longest x1 19.7 us: local(): whole_cols = lax.all_gather(regrouped, 'sp', axis=0, tiled=True)]
    dot_general x16 -> x0, matrix products: 19.6 us -> none  [the longest x3 3.65 us: hop(): jnp.einsum('dhkj,dhjv->dhkv', maps, states, precision=HIGHEST) + adds]
    all_to_all x1 -> x0, blocking collectives: 14.5 us -> none  [local(): lax.all_to_all(joined, 'fs', split_axis=1, concat_axis=0, tiled=True)]
    reduce_scatter x1 -> x0, waiting for transfers between devices: 6.31 us -> none  [local(): lax.psum_scatter(jnp.dot(lin_mix, lin_weight, preferred_element_type=jnp....]
    all_to_all x1 -> x0, starting transfers between devices: 3.71 us -> none  [local(): lax.all_to_all(outgoing, 'fs', split_axis=0, concat_axis=1, tiled=True)]
  transfers between devices with their start and end apart: 21 -> 0, of which waited for: 10 -> 0; matrix products, arithmetic and copies ran while one was open for 12% -> 0% of each run, Pallas kernels for 21% -> 0%
where the time goes in v1:
time: 109 us
  Pallas kernels  102 us (94%)
  local copies, waits for them, and re-layouts  6.23 us (6%)
    pallas_call x1, Pallas kernels, back(): pl.pallas_call(back_kernel, in_specs=[any_spec] * 3 + [pl.BlockSpec(memor...  54.9 us
    pallas_call x1, Pallas kernels, front(): pl.pallas_call(front_kernel, in_specs=[any_spec] * 9 + [vmem_spec] * 5, o...  47.4 us
    unnamed x9, local copies, waits for them, and re-layouts  5.49 us

profile of v1, /device:TPU:0, one launch (start us, length us, event | category | flops | bytes accessed | tf_op | source)
XLA Modules:
  0.0 108.6 jit_solution(18294360947797565458)
XLA Ops:
  0.0 0.0 copy-start
  0.0 0.9 copy.24
  0.9 0.9 copy.25
  1.8 0.7 copy.29.kv_ref
  2.6 0.0 copy-done
  2.6 0.0 copy-start.1
  2.6 1.0 copy.27.ddown_ref
  3.6 0.0 copy-done.1
  3.6 1.0 copy.28.edown_ref
  4.6 47.4 %front.1 = (bf16[512,640]{1,0:T(8,128)(2,1)}, f32[2,512,128]{2,1,0:T(8,128)}, f32[2,512,128]{2,1,0:T(8,128)}) custom-call(bf16[1,128,1024]{2,1,0:T(8,128)(2,1)} %x_ref.1, bf16[128,512]{1,0:T(8,128)(2,1)} %wr_ref.1, bf16[128,512]{1,0:T(8,128)(2,1)} %wk_ref.1, bf16[128,512]{1,0:T(8,128)(2,1)} %wv_ref.1, bf16[128,512]{1,0:T(8,128)(2,1)} %wq_ref.1, ...), custom_call_target="tpu_custom_call" | custom-call | tf_op jit(solution)/shard_map/front/pallas_call | solution.py:756
  52.0 54.9 %back.1 = bf16[1,64,2048]{2,1,0:T(8,128)(2,1)} custom-call(bf16[512,128]{1,0:T(8,128)(2,1)} %lin_ref.1, bf16[512,128]{1,0:T(8,128)(2,1)} %win_ref.1, f32[2,16,64,64]{3,2,1,0:T(8,128)} %init_ref.1, f32[1,16]{1,0:T(1,128)} %bitcast.11, bf16[512,640]{1,0:T(8,128)(2,1)} %get-tuple-element.8.proj_ref, f32[2,512,128]{2,1,0:T(8,128)} %get-tuple-element.9.log_ref, ...), custom_call_target="tpu_custom_call" | custom-call | tf_op jit(solution)/shard_map/back/pallas_call | solution.py:1328
  106.9 1.7 %copy.31 = bf16[1,64,2048]{2,1,0:T(8,128)(2,1)} copy(bf16[1,64,2048]{2,1,0:T(8,128)(2,1)} %back.1) | data formatting | bytes 524288
  (1 shorter events, 0.0 us)
Async XLA Ops:
  0.0 2.6 %copy-start = (bf16[2048,96]{0,1:T(8,128)(2,1)S(1)}, bf16[2048,96]{0,1:T(8,128)(2,1)}, u32[]{:S(2)}) copy-start(bf16[2048,96]{0,1:T(8,128)(2,1)} %param.29) | copy-start | bytes 1179652
  2.6 1.0 copy-start.1

commit v2 on v1

--- a/solution.py
+++ b/solution.py
@@ -439,371 +439,10 @@
     )
     return layer_out.astype(jnp.bfloat16)[None]
 
-MESH_IDS = pl.DeviceIdType.MESH
-
-
-def flipped(index, bits):
-    result = index
-    for bit in (1, 2):
-        if bits & bit:
-            result = result + bit - 2 * bit * lax.rem(lax.div(index, bit), 2)
-    return result
-
-
-def front_kernel(
-    x_ref,
-    wr_ref,
-    wk_ref,
-    wv_ref,
-    wq_ref,
-    kv_ref,
-    extra_ref,
-    dup_ref,
-    eup_ref,
-    gain_ref,
-    ddown_ref,
-    edown_ref,
-    doff_ref,
-    eoff_ref,
-    proj_ref,
-    log_ref,
-    learn_ref,
-    xbuf,
-    wbuf,
-    ebuf,
-    dup,
-    eup,
-    local_sem,
-    wlocal_sem,
-    up_send,
-    up_recv,
-    dn_send,
-    dn_recv,
-    sib_send,
-    sib_recv,
-    wz_send,
-    wz_recv,
-    e_send,
-    e_recv,
-    p_send,
-    p_recv,
-    f_send,
-    f_recv,
-):
-    sp, fs, tp = lax.axis_index("sp"), lax.axis_index("fs"), lax.axis_index("tp")
-    depth = lax.axis_size("sp")
-    width = lax.axis_size("fs")
-    tokens = x_ref.shape[1]
-    rows = wr_ref.shape[0]
-    sibling = {"tp": 1 - tp}
-    plane = ({"fs": flipped(fs, 1)}, {"fs": flipped(fs, 2)})
-
-    def remote(src, dst, send, recv, device):
-        return pltpu.make_async_remote_copy(
-            src_ref=src,
-            dst_ref=dst,
-            send_sem=send,
-            recv_sem=recv,
-            device_id=device,
-            device_id_type=MESH_IDS,
-        )
-
-    def rows_of(z, f):
-        return pl.ds(pl.multiple_of((z * width + f) * rows, rows), rows)
-
-    def pieces(z):
-        low = pl.ds(pl.multiple_of(z * PAIR, PAIR), PAIR)
-        shared = pl.ds(pl.multiple_of(lax.div(z, 2) * PAIR, PAIR), PAIR)
-        return [ref.at[:, low] for ref in (wr_ref, wk_ref, wv_ref, wq_ref)] + [
-            kv_ref.at[:, shared]
-        ]
-
-    def lanes(place):
-        return slice(place * PAIR, (place + 1) * PAIR)
-
-    cols = pl.ds(pl.multiple_of((tp * depth + sp) * PAIR, PAIR), PAIR)
-    own_x = pltpu.make_async_copy(x_ref.at[0], xbuf.at[sp, tp], local_sem.at[0])
-    own_x.start()
-    own_w = [
-        pltpu.make_async_copy(
-            piece, wbuf.at[rows_of(sp, fs), lanes(place)], wlocal_sem.at[place]
-        )
-        for place, piece in enumerate(pieces(sp))
-    ]
-    for copy in own_w:
-        copy.start()
-    small = [
-        pltpu.make_async_copy(extra_ref.at[0], ebuf.at[sp], local_sem.at[1]),
-        pltpu.make_async_copy(dup_ref.at[:, :, cols], dup, local_sem.at[2]),
-        pltpu.make_async_copy(eup_ref.at[:, :, cols], eup, local_sem.at[3]),
-    ]
-    for copy in small:
-        copy.start()
-
-    barrier = pltpu.get_barrier_semaphore()
-    peers = [{"sp": flipped(sp, k)} for k in range(1, depth)] + [sibling, *plane]
-    for peer in peers:
-        pl.semaphore_signal(barrier, inc=1, device_id=peer, device_id_type=MESH_IDS)
-    pl.semaphore_wait(barrier, len(peers))
-
-    def x_move(src_z, send, recv, device, src=None):
-        there = xbuf.at[src_z, tp]
-        return remote(there if src is None else src, there, send, recv, device)
-
-    up_to, dn_to = {"sp": sp + 1}, {"sp": sp - 1}
-
-    @pl.when(sp < depth - 1)
-    def _():
-        x_move(sp, up_send.at[0], up_recv.at[0], up_to, x_ref.at[0]).start()
-
-    @pl.when(sp > 0)
-    def _():
-        x_move(sp, dn_send.at[0], dn_recv.at[0], dn_to, x_ref.at[0]).start()
-
-    def wz_block(k):
-        there = wbuf.at[rows_of(sp, fs)]
-        return remote(there, there, wz_send.at[k - 1], wz_recv.at[k - 1], {"sp": flipped(sp, k)})
-
-    def e_block(k):
-        return remote(
-            extra_ref.at[0],
-            ebuf.at[sp],
-            e_send.at[k - 1],
-            e_recv.at[k - 1],
-            {"sp": flipped(sp, k)},
-        )
-
-    for k in range(1, depth):
-        target = flipped(sp, k)
-        for place, piece in enumerate(pieces(target)):
-            remote(
-                piece,
-                wbuf.at[rows_of(sp, fs), lanes(place)],
-                wz_send.at[k - 1],
-                wz_recv.at[k - 1],
-                {"sp": target},
-            ).start()
-        e_block(k).start()
-
-    own_x.wait()
-    sib = [x_move(sp, sib_send.at[0], sib_recv.at[0], sibling)]
-    sib[0].start()
-    for copy in own_w:
-        copy.wait()
-
-    def p_block(k, side):
-        there = wbuf.at[rows_of(flipped(sp, k), fs)]
-        return remote(there, there, p_send.at[k, side], p_recv.at[k, side], plane[side])
-
-    def f_block(k):
-        side = k % 2
-        there = wbuf.at[rows_of(flipped(sp, k), flipped(fs, 2 if side == 0 else 1))]
-        return remote(there, there, f_send.at[k], f_recv.at[k], plane[side])
-
-    def x_step(k):
-        @pl.when(sp >= k)
-        def _():
-            x_move(sp, up_send.at[k - 1], up_recv.at[k - 1], up_to).wait_recv()
-            if k < depth - 1:
-
-                @pl.when(sp < depth - 1)
-                def _():
-                    x_move(sp - k, up_send.at[k], up_recv.at[k], up_to).start()
-
-            x_move(sp - k, sib_send.at[k], sib_recv.at[k], sibling).start()
-
-        @pl.when(sp < depth - k)
-        def _():
-            x_move(sp, dn_send.at[k - 1], dn_recv.at[k - 1], dn_to).wait_recv()
-            if k < depth - 1:
-
-                @pl.when(sp > 0)
-                def _():
-                    x_move(sp + k, dn_send.at[k], dn_recv.at[k], dn_to).start()
-
-            x_move(sp + k, sib_send.at[depth + k - 1], sib_recv.at[depth + k - 1], sibling).start()
-
-    def w_step(k):
-        wz_block(k).wait_recv()
-        for side in range(2):
-            p_block(k, side).start()
-
-    def f_step(k):
-        for side in range(2):
-            p_block(k, side).wait_recv()
-        f_block(k).start()
-
-    for side in range(2):
-        p_block(0, side).start()
-    f_step(0)
-    x_step(1)
-    w_step(1)
-    w_step(2)
-    f_step(1)
-    x_step(2)
-    w_step(3)
-    f_step(2)
-    f_step(3)
-    x_step(3)
-    for k in range(depth):
-        f_block(k).wait_recv()
-    for k in range(1, depth):
-        e_block(k).wait_recv()
-    x_move(sp, sib_send.at[0], sib_recv.at[0], sibling).wait_recv()
-    for k in range(1, depth):
-
-        @pl.when(sp >= k)
-        def _():
-            x_move(sp, sib_send.at[k], sib_recv.at[k], sibling).wait_recv()
-
-        @pl.when(sp < depth - k)
-        def _():
-            place = depth + k - 1
-            x_move(sp, sib_send.at[place], sib_recv.at[place], sibling).wait_recv()
-
-    for copy in small:
-        copy.wait()
-
-    gain = gain_ref[...]
-    half = gain.shape[1] // 2
-    doff = doff_ref[:, cols]
-    eoff = eoff_ref[:, cols]
-
-    def block(z, carry):
-        parts = [xbuf[z, side].astype(F32) for side in range(2)]
-        total = sum(jnp.sum(part * part, axis=1, keepdims=True) for part in parts)
-        scale = lax.rsqrt(total / (2 * half) + NORM_EPS)
-        hidden = jnp.concatenate(
-            [
-                (part * scale * gain[:, side * half : (side + 1) * half]).astype(BF16)
-                for side, part in enumerate(parts)
-            ],
-            axis=1,
-        )
-        where = pl.ds(pl.multiple_of(z * tokens, tokens), tokens)
-
-        def dot(left, right):
-            return jnp.dot(left, right, preferred_element_type=F32)
-
-        proj_ref[where, :] = dot(hidden, wbuf[...]).astype(BF16)
-        decay_act = jnp.tanh(dot(hidden, ddown_ref[...]).astype(BF16).astype(F32)).astype(BF16)
-        learn_low = dot(hidden, edown_ref[...]).astype(BF16)
-        first_head = 2 * sp
-        spikes = jnp.concatenate(
-            [
-                jnp.broadcast_to(ebuf[z, pl.ds(first_head + head, 1), :], (HD, tokens))
-                for head in range(2)
-            ],
-            axis=0,
-        ).T
-        for direction in range(2):
-            pre = doff[direction : direction + 1] + dot(decay_act, dup[direction])
-            softplus = jnp.maximum(-pre, 0.0) + jnp.log1p(jnp.exp(-jnp.abs(pre)))
-            log_ref[direction, where, :] = spikes - jnp.exp(-softplus - 0.5)
-            learn = eoff[direction : direction + 1] + dot(learn_low, eup[direction])
-            learn_ref[direction, where, :] = jax.nn.sigmoid(learn)
-        return carry
-
-    lax.fori_loop(0, depth, block, 0)
-
-    @pl.when(sp < depth - 1)
-    def _():
-        x_move(sp, up_send.at[0], up_recv.at[0], up_to, x_ref.at[0]).wait_send()
-
-    @pl.when(sp > 0)
-    def _():
-        x_move(sp, dn_send.at[0], dn_recv.at[0], dn_to, x_ref.at[0]).wait_send()
-
-    x_move(sp, sib_send.at[0], sib_recv.at[0], sibling).wait_send()
-    for k in range(1, depth):
-
-        @pl.when(sp >= k)
-        def _():
-            x_move(sp, sib_send.at[k], sib_recv.at[k], sibling).wait_send()
-            if k < depth - 1:
-
-                @pl.when(sp < depth - 1)
-                def _():
-                    x_move(sp, up_send.at[k], up_recv.at[k], up_to).wait_send()
-
-        @pl.when(sp < depth - k)
-        def _():
-            place = depth + k - 1
-            x_move(sp, sib_send.at[place], sib_recv.at[place], sibling).wait_send()
-            if k < depth - 1:
-
-                @pl.when(sp > 0)
-                def _():
-                    x_move(sp, dn_send.at[k], dn_recv.at[k], dn_to).wait_send()
-
-        wz_block(k).wait_send()
-        e_block(k).wait_send()
-    for k in range(depth):
-        for side in range(2):
-            p_block(k, side).wait_send()
-        f_block(k).wait_send()
-
-
-def front(inputs, gain, weights, kv, extra, ddown, dup, doff, edown, eup, eoff):
-    depth = lax.axis_size("sp")
-    width = lax.axis_size("fs")
-    _, tokens, half = inputs.shape
-    total = tokens * depth
-    dma = pltpu.SemaphoreType.DMA
-    any_spec = pl.BlockSpec(memory_space=pl.ANY)
-    vmem_spec = pl.BlockSpec(memory_space=pltpu.VMEM)
-    low = ddown.shape[1]
-    return pl.pallas_call(
-        front_kernel,
-        in_specs=[any_spec] * 9 + [vmem_spec] * 5,
-        out_specs=[vmem_spec] * 3,
-        out_shape=[
-            jax.ShapeDtypeStruct((total, 5 * PAIR), BF16),
-            jax.ShapeDtypeStruct((2, total, PAIR), F32),
-            jax.ShapeDtypeStruct((2, total, PAIR), F32),
-        ],
-        scratch_shapes=[
-            pltpu.VMEM((depth, 2, tokens, half), BF16),
-            pltpu.VMEM((2 * half, 5 * PAIR), BF16),
-            pltpu.VMEM((depth, extra.shape[1], tokens), F32),
-            pltpu.VMEM((2, low, PAIR), BF16),
-            pltpu.VMEM((2, low, PAIR), BF16),
-            dma((4,)),
-            dma((5,)),
-            dma((depth,)),
-            dma((depth,)),
-            dma((depth,)),
-            dma((depth,)),
-            dma((2 * depth,)),
-            dma((2 * depth,)),
-            dma((depth - 1,)),
-            dma((depth - 1,)),
-            dma((depth - 1,)),
-            dma((depth - 1,)),
-            dma((width, 2)),
-            dma((width, 2)),
-            dma((width,)),
-            dma((width,)),
-        ],
-        compiler_params=pltpu.CompilerParams(collective_id=0, has_side_effects=True),
-        name="front",
-    )(
-        inputs,
-        *weights,
-        kv,
-        extra,
-        dup,
-        eup,
-        gain[None, :],
-        ddown,
-        edown,
-        doff,
-        eoff,
-    )
-
 
 SPAN = HD
 BATCH = 4
+VMEM_GRANT = 67_000_000
 QUAD = 4 * HD
 TN = (((0,), (0,)), ((), ()))
 
@@ -1136,95 +775,227 @@
     ]
 
 
-def back_kernel(
+MESH_IDS = pl.DeviceIdType.MESH
+
+
+def flipped(index, bits):
+    result = index
+    for bit in (1, 2):
+        if bits & bit:
+            result = result + bit - 2 * bit * lax.rem(lax.div(index, bit), 2)
+    return result
+
+
+def remote(src, dst, send, recv, device):
+    return pltpu.make_async_remote_copy(
+        src_ref=src,
+        dst_ref=dst,
+        send_sem=send,
+        recv_sem=recv,
+        device_id=device,
+        device_id_type=MESH_IDS,
+    )
+
+
+def layer_kernel(
+    x_ref,
+    wr_ref,
+    wk_ref,
+    wv_ref,
+    wq_ref,
+    extra_ref,
+    dup_ref,
+    eup_ref,
     lin_ref,
     win_ref,
     init_ref,
     sink_ref,
+    ak_ref,
+    av_ref,
+    gain_ref,
+    ddown_ref,
+    edown_ref,
+    doff_ref,
+    eoff_ref,
+    table_ref,
+    head_gain_ref,
+    out_ref,
+    xbuf,
+    wbuf,
+    kvbuf,
+    ebuf,
+    dup,
+    eup,
     proj_ref,
     log_ref,
     learn_ref,
-    table_ref,
-    gain_ref,
-    out_ref,
     owb,
     mbuf,
     mix_ref,
     init,
     local_sem,
-    z_send,
-    z_recv,
+    wlocal_sem,
+    up_send,
+    up_recv,
+    dn_send,
+    dn_recv,
+    sib_send,
+    sib_recv,
+    wz_send,
+    wz_recv,
+    e_send,
+    e_recv,
     p_send,
     p_recv,
     f_send,
     f_recv,
-    sib_send,
-    sib_recv,
+    oz_send,
+    oz_recv,
+    op_send,
+    op_recv,
+    of_send,
+    of_recv,
+    os_send,
+    os_recv,
     m_send,
     m_recv,
     *scratch,
 ):
     sp, fs, tp = lax.axis_index("sp"), lax.axis_index("fs"), lax.axis_index("tp")
-    depth = lax.axis_size("sp")
-    width = lax.axis_size("fs")
-    sides = lax.axis_size("tp")
-    rows, cols = lin_ref.shape
+    depth, width, sides = [lax.axis_size(axis) for axis in ("sp", "fs", "tp")]
+    tokens = x_ref.shape[1]
+    rows = wr_ref.shape[0]
+    out_rows, out_cols = lin_ref.shape
     share = out_ref.shape[1]
     sibling = {"tp": 1 - tp}
     plane = ({"fs": flipped(fs, 1)}, {"fs": flipped(fs, 2)})
-
-    def remote(src, dst, send, recv, device):
-        return pltpu.make_async_remote_copy(
-            src_ref=src,
-            dst_ref=dst,
-            send_sem=send,
-            recv_sem=recv,
-            device_id=device,
-            device_id_type=MESH_IDS,
-        )
+    up_to, dn_to = {"sp": sp + 1}, {"sp": sp - 1}
+
+    def rows_of(z, f):
+        return pl.ds(pl.multiple_of((z * width + f) * rows, rows), rows)
 
     def cols_of(z, f, many=1):
-        return pl.ds(pl.multiple_of((z * width + f) * cols, cols), many * cols)
-
-    local = [
+        return pl.ds(pl.multiple_of((z * width + f) * out_cols, out_cols), many * out_cols)
+
+    def pieces(z):
+        low = pl.ds(pl.multiple_of(z * PAIR, PAIR), PAIR)
+        return [ref.at[:, low] for ref in (wr_ref, wk_ref, wv_ref, wq_ref)]
+
+    def lanes(place):
+        return slice(place * PAIR, (place + 1) * PAIR)
+
+    cols = pl.ds(pl.multiple_of((tp * depth + sp) * PAIR, PAIR), PAIR)
+    head = (tp * depth + sp) * 2
+    own_x = pltpu.make_async_copy(x_ref.at[0], xbuf.at[sp, tp], local_sem.at[0])
+    own_w = [
         pltpu.make_async_copy(
-            ref, owb.at[tp, pl.ds(place * rows, rows), cols_of(sp, fs)], local_sem.at[place]
+            piece, wbuf.at[rows_of(sp, fs), lanes(place)], wlocal_sem.at[place]
+        )
+        for place, piece in enumerate(pieces(sp))
+    ]
+    own_o = [
+        pltpu.make_async_copy(
+            ref,
+            owb.at[tp, pl.ds(place * out_rows, out_rows), cols_of(sp, fs)],
+            local_sem.at[1 + place],
         )
         for place, ref in enumerate((lin_ref, win_ref))
     ]
-    head = (tp * depth + sp) * 2
-    local.append(pltpu.make_async_copy(init_ref.at[:, pl.ds(head, 2)], init, local_sem.at[2]))
-    for copy in local:
+    small = [
+        pltpu.make_async_copy(extra_ref.at[0], ebuf.at[sp], local_sem.at[3]),
+        pltpu.make_async_copy(dup_ref.at[:, :, cols], dup, local_sem.at[4]),
+        pltpu.make_async_copy(eup_ref.at[:, :, cols], eup, local_sem.at[5]),
+        pltpu.make_async_copy(init_ref.at[:, pl.ds(head, 2)], init, local_sem.at[6]),
+    ]
+    for copy in [own_x] + own_w + own_o + small:
         copy.start()
+    low_lanes = lax.broadcasted_iota(jnp.int32, (rows, PAIR), 1) < HD
+    near_key, near_value = ak_ref[...].astype(F32), av_ref[...].astype(F32)
+    packs = (
+        jnp.where(low_lanes, near_key, pltpu.roll(near_value, HD, 1)).astype(BF16),
+        jnp.where(low_lanes, pltpu.roll(near_key, HD, 1), near_value).astype(BF16),
+    )
+    for place, pack in enumerate(packs):
+        kvbuf[place] = pack
+    wbuf[rows_of(sp, fs), lanes(4)] = jnp.where(sp >= 2, packs[1], packs[0])
+
     barrier = pltpu.get_barrier_semaphore()
     pairs = [(k, t) for k in range(depth) for t in range(sides) if k or t]
     peers = [{"sp": flipped(sp, k), "tp": tp + t - 2 * t * tp} for k, t in pairs] + [*plane]
     for peer in peers:
         pl.semaphore_signal(barrier, inc=1, device_id=peer, device_id_type=MESH_IDS)
     pl.semaphore_wait(barrier, len(peers))
-    for copy in local:
-        copy.wait()
-
-    def z_block(k):
-        there = owb.at[tp, :, cols_of(sp, fs)]
-        return remote(there, there, z_send.at[k - 1], z_recv.at[k - 1], {"sp": flipped(sp, k)})
+
+    def x_move(src_z, send, recv, device, src=None):
+        there = xbuf.at[src_z, tp]
+        return remote(there if src is None else src, there, send, recv, device)
+
+    def wz_block(k):
+        there = wbuf.at[rows_of(sp, fs)]
+        return remote(there, there, wz_send.at[k - 1], wz_recv.at[k - 1], {"sp": flipped(sp, k)})
+
+    def e_block(k):
+        return remote(
+            extra_ref.at[0],
+            ebuf.at[sp],
+            e_send.at[k - 1],
+            e_recv.at[k - 1],
+            {"sp": flipped(sp, k)},
+        )
 
     def p_block(k, side):
-        there = owb.at[tp, :, cols_of(flipped(sp, k), fs)]
+        there = wbuf.at[rows_of(flipped(sp, k), fs)]
         return remote(there, there, p_send.at[k, side], p_recv.at[k, side], plane[side])
 
     def f_block(k):
         side = k % 2
+        there = wbuf.at[rows_of(flipped(sp, k), flipped(fs, 2 if side == 0 else 1))]
+        return remote(there, there, f_send.at[k], f_recv.at[k], plane[side])
+
+    def oz_block(k):
+        there = owb.at[tp, :, cols_of(sp, fs)]
+        return remote(there, there, oz_send.at[k - 1], oz_recv.at[k - 1], {"sp": flipped(sp, k)})
+
+    def op_block(k, side):
+        there = owb.at[tp, :, cols_of(flipped(sp, k), fs)]
+        return remote(there, there, op_send.at[k, side], op_recv.at[k, side], plane[side])
+
+    def of_block(k):
+        side = k % 2
         there = owb.at[tp, :, cols_of(flipped(sp, k), flipped(fs, 2 if side == 0 else 1))]
-        return remote(there, there, f_send.at[k], f_recv.at[k], plane[side])
-
-    def s_block(k):
+        return remote(there, there, of_send.at[k], of_recv.at[k], plane[side])
+
+    def os_block(k):
         there = owb.at[tp, :, cols_of(flipped(sp, k), 0, width)]
-        return remote(there, there, sib_send.at[k], sib_recv.at[k], sibling)
+        return remote(there, there, os_send.at[k], os_recv.at[k], sibling)
+
+    def x_step(k):
+        @pl.when(sp >= k)
+        def _():
+            x_move(sp, up_send.at[k - 1], up_recv.at[k - 1], up_to).wait_recv()
+            if k < depth - 1:
+
+                @pl.when(sp < depth - 1)
+                def _():
+                    x_move(sp - k, up_send.at[k], up_recv.at[k], up_to).start()
+
+            x_move(sp - k, sib_send.at[k], sib_recv.at[k], sibling).start()
+
+        @pl.when(sp < depth - k)
+        def _():
+            x_move(sp, dn_send.at[k - 1], dn_recv.at[k - 1], dn_to).wait_recv()
+            if k < depth - 1:
+
+                @pl.when(sp > 0)
+                def _():
+                    x_move(sp + k, dn_send.at[k], dn_recv.at[k], dn_to).start()
+
+            place = depth + k - 1
+            x_move(sp + k, sib_send.at[place], sib_recv.at[place], sibling).start()
 
     def w_step(k):
         if k:
-            z_block(k).wait_recv()
+            wz_block(k).wait_recv()
         for side in range(2):
             p_block(k, side).start()
 
@@ -1233,19 +1004,128 @@
             p_block(k, side).wait_recv()
         f_block(k).start()
 
-    def s_step(k):
+    def oz_start():
+        for k in range(1, depth):
+            oz_block(k).start()
+
+    def ow_step(k):
+        if k:
+            oz_block(k).wait_recv()
+        for side in range(2):
+            op_block(k, side).start()
+
+    def of_step(k):
+        for side in range(2):
+            op_block(k, side).wait_recv()
+        of_block(k).start()
+
+    def os_step(k):
+        of_block(k).wait_recv()
+        os_block(k).start()
+
+    @pl.when(sp < depth - 1)
+    def _():
+        x_move(sp, up_send.at[0], up_recv.at[0], up_to, x_ref.at[0]).start()
+
+    @pl.when(sp > 0)
+    def _():
+        x_move(sp, dn_send.at[0], dn_recv.at[0], dn_to, x_ref.at[0]).start()
+
+    for k in range(1, depth):
+        target = flipped(sp, k)
+        sources = pieces(target) + [kvbuf.at[lax.div(target, 2)]]
+        for place, piece in enumerate(sources):
+            remote(
+                piece,
+                wbuf.at[rows_of(sp, fs), lanes(place)],
+                wz_send.at[k - 1],
+                wz_recv.at[k - 1],
+                {"sp": target},
+            ).start()
+        e_block(k).start()
+    own_x.wait()
+    x_move(sp, sib_send.at[0], sib_recv.at[0], sibling).start()
+    for copy in own_w:
+        copy.wait()
+
+    w_step(0)
+    f_step(0)
+    x_step(1)
+    for copy in own_o:
+        copy.wait()
+    ow_step(0)
+    w_step(1)
+    w_step(2)
+    f_step(1)
+    x_step(2)
+    w_step(3)
+    f_step(2)
+    f_step(3)
+    x_step(3)
+    oz_start()
+    for k in range(depth):
         f_block(k).wait_recv()
-        s_block(k).start()
-
     for k in range(1, depth):
-        z_block(k).start()
-    w_step(0)
+        e_block(k).wait_recv()
+    x_move(sp, sib_send.at[0], sib_recv.at[0], sibling).wait_recv()
+    for k in range(1, depth):
+
+        @pl.when(sp >= k)
+        def _():
+            x_move(sp, sib_send.at[k], sib_recv.at[k], sibling).wait_recv()
+
+        @pl.when(sp < depth - k)
+        def _():
+            place = depth + k - 1
+            x_move(sp, sib_send.at[place], sib_recv.at[place], sibling).wait_recv()
+
+    for copy in small:
+        copy.wait()
+
+    gain = gain_ref[...]
+    half = gain.shape[1] // 2
+    doff = doff_ref[:, cols]
+    eoff = eoff_ref[:, cols]
+
+    def block(z, carry):
+        parts = [xbuf[z, side].astype(F32) for side in range(2)]
+        total = sum(jnp.sum(part * part, axis=1, keepdims=True) for part in parts)
+        scale = lax.rsqrt(total / (2 * half) + NORM_EPS)
+        hidden = jnp.concatenate(
+            [
+                (part * scale * gain[:, side * half : (side + 1) * half]).astype(BF16)
+                for side, part in enumerate(parts)
+            ],
+            axis=1,
+        )
+        where = pl.ds(pl.multiple_of(z * tokens, tokens), tokens)
+        proj_ref[where, :] = mm(hidden, wbuf[...]).astype(BF16)
+        decay_low = mm(hidden, ddown_ref[...], NT).astype(BF16)
+        decay_act = jnp.tanh(decay_low.astype(F32)).astype(BF16)
+        learn_low = mm(hidden, edown_ref[...], NT).astype(BF16)
+        spikes = jnp.concatenate(
+            [
+                jnp.broadcast_to(ebuf[z, pl.ds(2 * sp + place, 1), :], (HD, tokens))
+                for place in range(2)
+            ],
+            axis=0,
+        ).T
+        for direction in range(2):
+            pre = doff[direction : direction + 1] + mm(decay_act, dup[direction])
+            softplus = jnp.maximum(-pre, 0.0) + jnp.log1p(jnp.exp(-jnp.abs(pre)))
+            log_ref[direction, where, :] = spikes - jnp.exp(-softplus - 0.5)
+            learn = eoff[direction : direction + 1] + mm(learn_low, eup[direction])
+            learn_ref[direction, where, :] = jax.nn.sigmoid(learn)
+        return carry
+
+    lax.fori_loop(0, depth, block, 0)
+
     plan = [
-        [(f_step, 0), (w_step, 1)],
-        [(s_step, 0), (w_step, 2)],
-        [(f_step, 1)],
-        [(w_step, 3), (s_step, 1)],
-        [(f_step, 2)],
+        [(of_step, 0), (ow_step, 1)],
+        [(os_step, 0)],
+        [(ow_step, 2)],
+        [(of_step, 1)],
+        [(ow_step, 3), (os_step, 1), (of_step, 2)],
     ]
     queue = iter(plan)
 
@@ -1254,14 +1134,13 @@
             step(k)
 
     states = jnp.concatenate([init[d, h] for d in range(2) for h in range(2)], axis=1)
-    lanes = pl.ds(pl.multiple_of((tp * depth + sp) * PAIR, PAIR), PAIR)
     mix_body(
         hook,
         proj_ref,
         log_ref,
         learn_ref,
         table_ref,
-        gain_ref[:, lanes],
+        head_gain_ref[:, cols],
         [sink_ref[0, head], sink_ref[0, head + 1]],
         states,
         mix_ref,
@@ -1283,9 +1162,8 @@
         m_block(k, t).start()
     mine = sp * sides + tp
     mbuf[mine] = mix_ref[pl.ds(pl.multiple_of(mine * share, share), share), :]
-    f_step(3)
-    s_step(2)
-    s_step(3)
+    of_step(3)
+    os_step(2)
     for k, t in pairs:
         m_block(k, t).wait_recv()
     lefts = [
@@ -1297,72 +1175,56 @@
         for side in range(sides)
     ]
     for k in range(depth):
-        s_block(k).wait_recv()
+        if k == depth - 1:
+            os_step(k)
+        os_block(k).wait_recv()
         span = cols_of(flipped(sp, k), 0, width)
         out_ref[0, :, span] = sum(
-            jnp.dot(lefts[side], owb[side, :, span], preferred_element_type=F32)
-            for side in range(sides)
+            mm(lefts[side], owb[side, :, span]) for side in range(sides)
         ).astype(BF16)
+
+    @pl.when(sp < depth - 1)
+    def _():
+        x_move(sp, up_send.at[0], up_recv.at[0], up_to, x_ref.at[0]).wait_send()
+
+    @pl.when(sp > 0)
+    def _():
+        x_move(sp, dn_send.at[0], dn_recv.at[0], dn_to, x_ref.at[0]).wait_send()
+
+    x_move(sp, sib_send.at[0], sib_recv.at[0], sibling).wait_send()
+    for k in range(1, depth):
+
+        @pl.when(sp >= k)
+        def _():
+            x_move(sp, sib_send.at[k], sib_recv.at[k], sibling).wait_send()
+            if k < depth - 1:
+
+                @pl.when(sp < depth - 1)
+                def _():
+                    x_move(sp, up_send.at[k], up_recv.at[k], up_to).wait_send()
+
+        @pl.when(sp < depth - k)
+        def _():
+            place = depth + k - 1
+            x_move(sp, sib_send.at[place], sib_recv.at[place], sibling).wait_send()
+            if k < depth - 1:
+
+                @pl.when(sp > 0)
+                def _():
+                    x_move(sp, dn_send.at[k], dn_recv.at[k], dn_to).wait_send()
+
+        wz_block(k).wait_send()
+        e_block(k).wait_send()
+        oz_block(k).wait_send()
     for k in range(depth):
-        if k:
-            z_block(k).wait_send()
         for side in range(2):
             p_block(k, side).wait_send()
+            op_block(k, side).wait_send()
         f_block(k).wait_send()
-        s_block(k).wait_send()
+        of_block(k).wait_send()
+        os_block(k).wait_send()
     for k, t in pairs:
         m_block(k, t).wait_send()
-
-
-def back(proj, logs, learn, gain, sink, init, lin_weight, win_weight):
-    depth = lax.axis_size("sp")
-    width = lax.axis_size("fs")
-    sides = lax.axis_size("tp")
-    total = proj.shape[0]
-    rows, cols = lin_weight.shape
-    share = total // (depth * sides)
-    dma = pltpu.SemaphoreType.DMA
-    any_spec = pl.BlockSpec(memory_space=pl.ANY)
-    vmem_spec = pl.BlockSpec(memory_space=pltpu.VMEM)
-    features = cols * depth * width
-    return pl.pallas_call(
-        back_kernel,
-        in_specs=[any_spec] * 3 + [pl.BlockSpec(memory_space=pltpu.SMEM)] + [vmem_spec] * 5,
-        out_specs=vmem_spec,
-        out_shape=jax.ShapeDtypeStruct((1, share, features), BF16),
-        scratch_shapes=[
-            pltpu.VMEM((sides, 2 * rows, features), BF16),
-            pltpu.VMEM((depth * sides, share, 2 * PAIR), BF16),
-            pltpu.VMEM((total, 2 * PAIR), BF16),
-            pltpu.VMEM((2, 2, HD, HD), F32),
-            dma((3,)),
-            dma((depth - 1,)),
-            dma((depth - 1,)),
-            dma((depth, 2)),
-            dma((depth, 2)),
-            dma((depth,)),
-            dma((depth,)),
-            dma((depth,)),
-            dma((depth,)),
-            dma((depth * sides,)),
-            dma((depth * sides,)),
-        ]
-        + mix_scratch(total),
-        compiler_params=pltpu.CompilerParams(
-            collective_id=1, has_side_effects=True, vmem_limit_bytes=60 * 2**20
-        ),
-        name="back",
-    )(
-        lin_weight,
-        win_weight,
-        init,
-        sink[None, :],
-        proj,
-        logs,
-        learn,
-        jnp.asarray(rope_tables(total)),
-        gain[None, :],
-    )
 
 
 def by_heads(
@@ -1387,36 +1249,90 @@
     linear_output_weight,
     window_output_weight,
 ):
-    count = window_key_weight.shape[0]
-    kv = jnp.concatenate(
-        [
-            weight.reshape(count, -1, HD)
-            for weight in (window_key_weight, window_value_weight)
-        ],
-        axis=2,
-    ).reshape(count, -1)
-    proj, logs, learn = front(
+    depth, width, sides = [lax.axis_size(axis) for axis in ("sp", "fs", "tp")]
+    _, tokens, half = inputs.shape
+    total = tokens * depth
+    rows = receptance_weight.shape[0]
+    out_rows, out_cols = linear_output_weight.shape
+    features = out_cols * depth * width
+    share = tokens // sides
+    low = decay_down_weight.shape[1]
+    dma = pltpu.SemaphoreType.DMA
+    any_spec = pl.BlockSpec(memory_space=pl.ANY)
+    vmem_spec = pl.BlockSpec(memory_space=pltpu.VMEM)
+    return pl.pallas_call(
+        layer_kernel,
+        in_specs=[any_spec] * 11 + [pl.BlockSpec(memory_space=pltpu.SMEM)] + [vmem_spec] * 9,
+        out_specs=vmem_spec,
+        out_shape=jax.ShapeDtypeStruct((1, share, features), BF16),
+        scratch_shapes=[
+            pltpu.VMEM((depth, 2, tokens, half), BF16),
+            pltpu.VMEM((2 * half, 5 * PAIR), BF16),
+            pltpu.VMEM((2, rows, PAIR), BF16),
+            pltpu.VMEM((depth, decay_log_extra.shape[1], tokens), F32),
+            pltpu.VMEM((2, low, PAIR), BF16),
+            pltpu.VMEM((2, low, PAIR), BF16),
+            pltpu.VMEM((total, 5 * PAIR), BF16),
+            pltpu.VMEM((2, total, PAIR), F32),
+            pltpu.VMEM((2, total, PAIR), F32),
+            pltpu.VMEM((sides, 2 * out_rows, features), BF16),
+            pltpu.VMEM((depth * sides, share, 2 * PAIR), BF16),
+            pltpu.VMEM((total, 2 * PAIR), BF16),
+            pltpu.VMEM((2, 2, HD, HD), F32),
+            dma((7,)),
+            dma((4,)),
+            dma((depth,)),
+            dma((depth,)),
+            dma((depth,)),
+            dma((depth,)),
+            dma((2 * depth,)),
+            dma((2 * depth,)),
+            dma((depth - 1,)),
+            dma((depth - 1,)),
+            dma((depth - 1,)),
+            dma((depth - 1,)),
+            dma((width, 2)),
+            dma((width, 2)),
+            dma((width,)),
+            dma((width,)),
+            dma((depth - 1,)),
+            dma((depth - 1,)),
+            dma((depth, 2)),
+            dma((depth, 2)),
+            dma((depth,)),
+            dma((depth,)),
+            dma((depth,)),
+            dma((depth,)),
+            dma((depth * sides,)),
+            dma((depth * sides,)),
+        ]
+        + mix_scratch(total),
+        compiler_params=pltpu.CompilerParams(
+            collective_id=0, has_side_effects=True, vmem_limit_bytes=VMEM_GRANT
+        ),
+        name="layer",
+    )(
         inputs,
-        input_norm_gain,
-        (receptance_weight, linear_key_weight, linear_value_weight, window_query_weight),
-        kv,
+        receptance_weight,
+        linear_key_weight,
+        linear_value_weight,
+        window_query_weight,
         decay_log_extra,
-        decay_down_weight,
         decay_up_weight,
-        decay_offset,
-        erasure_down_weight,
         erasure_up_weight,
-        erasure_offset,
-    )
-    return back(
-        proj,
-        logs,
-        learn,
-        head_norm_gain,
-        query_sink_logit,
-        initial_state,
         linear_output_weight,
         window_output_weight,
+        initial_state,
+        query_sink_logit[None, :],
+        window_key_weight,
+        window_value_weight,
+        input_norm_gain[None, :],
+        decay_down_weight.T,
+        erasure_down_weight.T,
+        decay_offset,
+        erasure_offset,
+        jnp.asarray(rope_tables(total)),
+        head_norm_gain[None, :],
     )
 
 

time: 109 us -> 96.4 us (0.88)
  Pallas kernels: 102 us -> 94.5 us
  local copies, waits for them, and re-layouts: 6.23 us -> 1.67 us
    pallas_call x2 -> x1, Pallas kernels: 102 us -> 94.5 us  [by_heads(): pl.pallas_call(layer_kernel, in_specs=[any_spec] * 11 + [pl.BlockSpec(mem...]
    unnamed x9 -> x1, local copies, waits for them, and re-layouts: 5.49 us -> 1.67 us
where the time goes in v2:
time: 96.4 us; the launch traced here: 96.2 us
  Pallas kernels  94.5 us (98%)
  local copies, waits for them, and re-layouts  1.67 us (2%)
    pallas_call x1, Pallas kernels, by_heads(): pl.pallas_call(layer_kernel, in_specs=[any_spec] * 11 + [pl.BlockSpec(mem...  94.5 us

profile of v2, /device:TPU:0, one launch (start us, length us, event | category | flops | bytes accessed | tf_op | source)
XLA Modules:
  0.0 96.2 jit_solution(6383981832410169742)
XLA Ops:
  0.0 94.5 %layer.1 = bf16[1,64,2048]{2,1,0:T(8,128)(2,1)} custom-call(bf16[1,128,1024]{2,1,0:T(8,128)(2,1)} %x_ref.1, bf16[128,512]{1,0:T(8,128)(2,1)} %wr_ref.1, bf16[128,512]{1,0:T(8,128)(2,1)} %wk_ref.1, bf16[128,512]{1,0:T(8,128)(2,1)} %wv_ref.1, bf16[128,512]{1,0:T(8,128)(2,1)} %wq_ref.1, f32[1,8,128]{2,1,0:T(8,128)} %extra_ref.1, bf16[2,96,1024]{2,1,0:T(8,128)(2,1)} %dup_ref.1, ...), custom_call_target="tpu_custom_call" | custom-call | tf_op jit(solution)/shard_map/layer/pallas_call | solution.py:1263
  94.5 1.7 %copy.23 = bf16[1,64,2048]{2,1,0:T(8,128)(2,1)} copy(bf16[1,64,2048]{2,1,0:T(8,128)(2,1)} %layer.1) | data formatting | bytes 524288

commit v3 on v2

--- a/solution.py
+++ b/solution.py
@@ -441,7 +441,8 @@
 
 
 SPAN = HD
-BATCH = 4
+PARTS = 2
+ORDER = (1, 3, 2)
 VMEM_GRANT = 67_000_000
 QUAD = 4 * HD
 TN = (((0,), (0,)), ((), ()))
@@ -580,8 +581,7 @@
     def both(one, other):
         return jnp.concatenate([one, other], axis=1)
 
-    def batch(index, carry, size):
-        groups = [index * size + k for k in range(size)]
+    def batch(groups):
         erased, seens, read_eraseds, starts, lefts, finals, spans, values = [], [], [], [], [], [], [], []
         for group in groups:
             rows = (rows_at(group), rows_at(count - 1 - group))
@@ -612,6 +612,7 @@
             firsts = [single(solve, jnp.where(at, one, 0.0)) for solve, one in zip(solves, erased)]
             solves = [solve - single(one, solve) for solve, one in zip(solves, firsts)]
             width *= 2
+        hook()
         misses = [
             eye - solve - quad_dot([one], solve)[0] for solve, one in zip(solves, erased)
         ]
@@ -644,12 +645,13 @@
             s_a[group] = (gained[:SPAN] + gained[SPAN : 2 * SPAN]) + (
                 gained[2 * SPAN : 3 * SPAN] + gained[3 * SPAN :]
             )
-        return carry
-
-    size = min(BATCH, count)
-    for index in range(count // size):
-        batch(index, 0, size)
-        hook()
+
+    size = count // 2
+    middle = range(count // 4, count - count // 4)
+    batch(list(middle))
+    hook()
+    batch([group for group in range(count) if group not in middle])
+    hook()
 
     def advance(group, state):
         high, low = halves(state)
@@ -679,8 +681,9 @@
             carry = finish(index * size + k, carry)
         return carry
 
-    lax.fori_loop(0, count // size, finish_batch, 0)
-    hook()
+    for index in range(count // size):
+        finish_batch(index, 0)
+        hook()
 
     quarter = HD // 4
     back = lax.rem(lane, 2 * quarter) >= quarter
@@ -718,6 +721,7 @@
         return carry
 
     lax.fori_loop(0, grid, turn, 0)
+    hook()
     reach = ATT_BLOCK + 2 * WINDOW
     ahead_of = lax.broadcasted_iota(jnp.int32, (ATT_BLOCK, reach), 1) - (
         WINDOW + lax.broadcasted_iota(jnp.int32, (ATT_BLOCK, reach), 0)
@@ -745,8 +749,10 @@
         mix_ref[rows, PAIR:] = jnp.where(mine, mixed[0], mixed[1]).astype(BF16)
         return carry
 
-    lax.fori_loop(0, total // ATT_BLOCK, attend, 0)
-    hook()
+    blocks = total // ATT_BLOCK
+    for part in range(2):
+        lax.fori_loop(part * blocks // 2, (part + 1) * blocks // 2, attend, 0)
+        hook()
 
     def norm(place, carry):
         rows = rows_at(place)
@@ -832,6 +838,7 @@
     owb,
     mbuf,
     mix_ref,
+    lbuf,
     init,
     local_sem,
     wlocal_sem,
@@ -849,8 +856,10 @@
     p_recv,
     f_send,
     f_recv,
-    oz_send,
-    oz_recv,
+    ou_send,
+    ou_recv,
+    od_send,
+    od_recv,
     op_send,
     op_recv,
     of_send,
@@ -926,9 +935,33 @@
         pl.semaphore_signal(barrier, inc=1, device_id=peer, device_id_type=MESH_IDS)
     pl.semaphore_wait(barrier, len(peers))
 
-    def x_move(src_z, send, recv, device, src=None):
-        there = xbuf.at[src_z, tp]
-        return remote(there if src is None else src, there, send, recv, device)
+    up_exists, dn_exists = sp < depth - 1, sp > 0
+
+    def at_distance(k, body):
+        if k == 0:
+            body(sp)
+            return
+
+        def one(j, carry):
+            body(sp + (2 * j - 1) * k)
+            return carry
+
+        lax.fori_loop(jnp.where(sp >= k, 0, 1), jnp.where(sp < depth - k, 2, 1), one, 0)
+
+    def x_move(z, part, send, recv, device, src=None):
+        span = pl.ds(part * (tokens // PARTS), tokens // PARTS)
+        there = xbuf.at[z, tp, span]
+        return remote(there if src is None else src.at[0, span], there, send, recv, device)
+
+    def x_up(z, k, part, src=None):
+        return x_move(z, part, up_send.at[k, part], up_recv.at[k, part], up_to, src)
+
+    def x_dn(z, k, part, src=None):
+        return x_move(z, part, dn_send.at[k, part], dn_recv.at[k, part], dn_to, src)
+
+    def sib_move(z):
+        there = xbuf.at[z, tp]
+        return remote(there, there, sib_send.at[z], sib_recv.at[z], sibling)
 
     def wz_block(k):
         there = wbuf.at[rows_of(sp, fs)]
@@ -952,46 +985,64 @@
         there = wbuf.at[rows_of(flipped(sp, k), flipped(fs, 2 if side == 0 else 1))]
         return remote(there, there, f_send.at[k], f_recv.at[k], plane[side])
 
-    def oz_block(k):
-        there = owb.at[tp, :, cols_of(sp, fs)]
-        return remote(there, there, oz_send.at[k - 1], oz_recv.at[k - 1], {"sp": flipped(sp, k)})
-
-    def op_block(k, side):
-        there = owb.at[tp, :, cols_of(flipped(sp, k), fs)]
-        return remote(there, there, op_send.at[k, side], op_recv.at[k, side], plane[side])
-
-    def of_block(k):
-        side = k % 2
-        there = owb.at[tp, :, cols_of(flipped(sp, k), flipped(fs, 2 if side == 0 else 1))]
-        return remote(there, there, of_send.at[k], of_recv.at[k], plane[side])
-
-    def os_block(k):
-        there = owb.at[tp, :, cols_of(flipped(sp, k), 0, width)]
-        return remote(there, there, os_send.at[k], os_recv.at[k], sibling)
+    def o_move(z, send, recv, device):
+        there = owb.at[tp, :, cols_of(z, fs)]
+        return remote(there, there, send, recv, device)
+
+    def o_up(z, k):
+        return o_move(z, ou_send.at[k], ou_recv.at[k], up_to)
+
+    def o_dn(z, k):
+        return o_move(z, od_send.at[k], od_recv.at[k], dn_to)
+
+    def op_block(z, side):
+        return o_move(z, op_send.at[z, side], op_recv.at[z, side], plane[side])
+
+    def of_block(z):
+        odd = lax.rem(z, 2)
+        near, far = flipped(fs, 1), flipped(fs, 2)
+        there = owb.at[tp, :, cols_of(z, far + odd * (near - far))]
+        device = {"fs": near + odd * (far - near)}
+        return remote(there, there, of_send.at[z], of_recv.at[z], device)
+
+    def os_block(z):
+        there = owb.at[tp, :, cols_of(z, 0, width)]
+        return remote(there, there, os_send.at[z], os_recv.at[z], sibling)
 
     def x_step(k):
-        @pl.when(sp >= k)
-        def _():
-            x_move(sp, up_send.at[k - 1], up_recv.at[k - 1], up_to).wait_recv()
-            if k < depth - 1:
-
-                @pl.when(sp < depth - 1)
-                def _():
-                    x_move(sp - k, up_send.at[k], up_recv.at[k], up_to).start()
-
-            x_move(sp - k, sib_send.at[k], sib_recv.at[k], sibling).start()
-
-        @pl.when(sp < depth - k)
-        def _():
-            x_move(sp, dn_send.at[k - 1], dn_recv.at[k - 1], dn_to).wait_recv()
-            if k < depth - 1:
-
-                @pl.when(sp > 0)
-                def _():
-                    x_move(sp + k, dn_send.at[k], dn_recv.at[k], dn_to).start()
-
-            place = depth + k - 1
-            x_move(sp + k, sib_send.at[place], sib_recv.at[place], sibling).start()
+        for part in range(PARTS):
+
+            @pl.when(sp >= k)
+            def _():
+                x_up(sp, k - 1, part).wait_recv()
+                if k < depth - 1:
+
+                    @pl.when(up_exists)
+                    def _():
+                        x_up(sp - k, k, part).start()
+
+            @pl.when(sp < depth - k)
+            def _():
+                x_dn(sp, k - 1, part).wait_recv()
+                if k < depth - 1:
+
+                    @pl.when(dn_exists)
+                    def _():
+                        x_dn(sp + k, k, part).start()
+
+        at_distance(k, lambda z: sib_move(z).start())
+        o_own(k)
+
+    def o_own(k):
+        if k < depth - 1:
+
+            @pl.when(sp == k)
+            def _():
+                o_up(sp, 0).start()
+
+            @pl.when(sp == depth - 1 - k)
+            def _():
+                o_dn(sp, 0).start()
 
     def w_step(k):
         if k:
@@ -1004,34 +1055,47 @@
             p_block(k, side).wait_recv()
         f_block(k).start()
 
-    def oz_start():
-        for k in range(1, depth):
-            oz_block(k).start()
-
-    def ow_step(k):
-        if k:
-            oz_block(k).wait_recv()
+    def op_start(z):
         for side in range(2):
-            op_block(k, side).start()
+            op_block(z, side).start()
+
+    def o_step(k):
+        @pl.when(sp >= k)
+        def _():
+            o_up(sp, k - 1).wait_recv()
+            if k < depth - 1:
+
+                @pl.when(up_exists)
+                def _():
+                    o_up(sp - k, k).start()
+
+        @pl.when(sp < depth - k)
+        def _():
+            o_dn(sp, k - 1).wait_recv()
+            if k < depth - 1:
+
+                @pl.when(dn_exists)
+                def _():
+                    o_dn(sp + k, k).start()
+
+        at_distance(k, op_start)
 
     def of_step(k):
-        for side in range(2):
-            op_block(k, side).wait_recv()
-        of_block(k).start()
+        def body(z):
+            for side in range(2):
+                op_block(z, side).wait_recv()
+            of_block(z).start()
+
+        at_distance(k, body)
 
     def os_step(k):
-        of_block(k).wait_recv()
-        os_block(k).start()
-
-    @pl.when(sp < depth - 1)
-    def _():
-        x_move(sp, up_send.at[0], up_recv.at[0], up_to, x_ref.at[0]).start()
-
-    @pl.when(sp > 0)
-    def _():
-        x_move(sp, dn_send.at[0], dn_recv.at[0], dn_to, x_ref.at[0]).start()
-
-    for k in range(1, depth):
+        def body(z):
+            of_block(z).wait_recv()
+            os_block(z).start()
+
+        at_distance(k, body)
+
+    for k in ORDER:
         target = flipped(sp, k)
         sources = pieces(target) + [kvbuf.at[lax.div(target, 2)]]
         for place, piece in enumerate(sources):
@@ -1043,42 +1107,39 @@
                 {"sp": target},
             ).start()
         e_block(k).start()
-    own_x.wait()
-    x_move(sp, sib_send.at[0], sib_recv.at[0], sibling).start()
     for copy in own_w:
         copy.wait()
-
     w_step(0)
-    f_step(0)
-    x_step(1)
+    for part in range(PARTS):
+
+        @pl.when(up_exists)
+        def _():
+            x_up(sp, 0, part, x_ref).start()
+
+        @pl.when(dn_exists)
+        def _():
+            x_dn(sp, 0, part, x_ref).start()
+
+    own_x.wait()
+    sib_move(sp).start()
     for copy in own_o:
         copy.wait()
-    ow_step(0)
-    w_step(1)
-    w_step(2)
+    o_own(0)
+    f_step(0)
+    for k in ORDER:
+        w_step(k)
     f_step(1)
+    f_step(3)
+    x_step(1)
+    f_step(2)
+    op_start(sp)
     x_step(2)
-    w_step(3)
-    f_step(2)
-    f_step(3)
     x_step(3)
-    oz_start()
+    of_step(0)
     for k in range(depth):
         f_block(k).wait_recv()
     for k in range(1, depth):
         e_block(k).wait_recv()
-    x_move(sp, sib_send.at[0], sib_recv.at[0], sibling).wait_recv()
-    for k in range(1, depth):
-
-        @pl.when(sp >= k)
-        def _():
-            x_move(sp, sib_send.at[k], sib_recv.at[k], sibling).wait_recv()
-
-        @pl.when(sp < depth - k)
-        def _():
-            place = depth + k - 1
-            x_move(sp, sib_send.at[place], sib_recv.at[place], sibling).wait_recv()
-
     for copy in small:
         copy.wait()
 
@@ -1087,7 +1148,8 @@
     doff = doff_ref[:, cols]
     eoff = eoff_ref[:, cols]
 
-    def block(z, carry):
+    def block(z):
+        sib_move(z).wait_recv()
         parts = [xbuf[z, side].astype(F32) for side in range(2)]
         total = sum(jnp.sum(part * part, axis=1, keepdims=True) for part in parts)
         scale = lax.rsqrt(total / (2 * half) + NORM_EPS)
@@ -1116,16 +1178,23 @@
             log_ref[direction, where, :] = spikes - jnp.exp(-softplus - 0.5)
             learn = eoff[direction : direction + 1] + mm(learn_low, eup[direction])
             learn_ref[direction, where, :] = jax.nn.sigmoid(learn)
-        return carry
-
-    lax.fori_loop(0, depth, block, 0)
+
+    for k in range(depth):
+        at_distance(k, block)
+        if k == 1:
+            o_step(1)
 
     plan = [
-        [(of_step, 0), (ow_step, 1)],
-        [(os_step, 0)],
-        [(ow_step, 2)],
-        [(of_step, 1)],
-        [(ow_step, 3), (os_step, 1), (of_step, 2)],
+        [],
+        [(os_step, 0), (o_step, 2)],
+        [],
+        [],
+        [],
+        [(of_step, 1), (o_step, 3)],
+        [],
+        [],
+        [(of_step, 2)],
+        [],
     ]
     queue = iter(plan)
 
@@ -1162,6 +1231,7 @@
         m_block(k, t).start()
     mine = sp * sides + tp
     mbuf[mine] = mix_ref[pl.ds(pl.multiple_of(mine * share, share), share), :]
+    os_step(1)
     of_step(3)
     os_step(2)
     for k, t in pairs:
@@ -1174,48 +1244,39 @@
         )
         for side in range(sides)
     ]
-    for k in range(depth):
-        if k == depth - 1:
-            os_step(k)
-        os_block(k).wait_recv()
-        span = cols_of(flipped(sp, k), 0, width)
+    for side in range(sides):
+        lbuf[side] = lefts[side]
+
+    def product(z):
+        os_block(z).wait_recv()
+        span = cols_of(z, 0, width)
         out_ref[0, :, span] = sum(
-            mm(lefts[side], owb[side, :, span]) for side in range(sides)
+            mm(lbuf[side], owb[side, :, span]) for side in range(sides)
         ).astype(BF16)
 
-    @pl.when(sp < depth - 1)
-    def _():
-        x_move(sp, up_send.at[0], up_recv.at[0], up_to, x_ref.at[0]).wait_send()
-
-    @pl.when(sp > 0)
-    def _():
-        x_move(sp, dn_send.at[0], dn_recv.at[0], dn_to, x_ref.at[0]).wait_send()
-
-    x_move(sp, sib_send.at[0], sib_recv.at[0], sibling).wait_send()
+    at_distance(0, product)
+    at_distance(1, product)
+    at_distance(2, product)
+    os_step(3)
+    at_distance(3, product)
+
+    for k in range(depth - 1):
+
+        @pl.when((sp >= k) & up_exists)
+        def _():
+            for part in range(PARTS):
+                x_up(sp, k, part).wait_send()
+            o_up(sp, k).wait_send()
+
+        @pl.when((sp < depth - k) & dn_exists)
+        def _():
+            for part in range(PARTS):
+                x_dn(sp, k, part).wait_send()
+            o_dn(sp, k).wait_send()
+
     for k in range(1, depth):
-
-        @pl.when(sp >= k)
-        def _():
-            x_move(sp, sib_send.at[k], sib_recv.at[k], sibling).wait_send()
-            if k < depth - 1:
-
-                @pl.when(sp < depth - 1)
-                def _():
-                    x_move(sp, up_send.at[k], up_recv.at[k], up_to).wait_send()
-
-        @pl.when(sp < depth - k)
-        def _():
-            place = depth + k - 1
-            x_move(sp, sib_send.at[place], sib_recv.at[place], sibling).wait_send()
-            if k < depth - 1:
-
-                @pl.when(sp > 0)
-                def _():
-                    x_move(sp, dn_send.at[k], dn_recv.at[k], dn_to).wait_send()
-
         wz_block(k).wait_send()
         e_block(k).wait_send()
-        oz_block(k).wait_send()
     for k in range(depth):
         for side in range(2):
             p_block(k, side).wait_send()
@@ -1223,6 +1284,7 @@
         f_block(k).wait_send()
         of_block(k).wait_send()
         os_block(k).wait_send()
+        sib_move(k).wait_send()
     for k, t in pairs:
         m_block(k, t).wait_send()
 
@@ -1278,15 +1340,16 @@
             pltpu.VMEM((sides, 2 * out_rows, features), BF16),
             pltpu.VMEM((depth * sides, share, 2 * PAIR), BF16),
             pltpu.VMEM((total, 2 * PAIR), BF16),
+            pltpu.VMEM((sides, share, 2 * out_rows), BF16),
             pltpu.VMEM((2, 2, HD, HD), F32),
             dma((7,)),
             dma((4,)),
+            dma((depth, PARTS)),
+            dma((depth, PARTS)),
+            dma((depth, PARTS)),
+            dma((depth, PARTS)),
             dma((depth,)),
             dma((depth,)),
-            dma((depth,)),
-            dma((depth,)),
-            dma((2 * depth,)),
-            dma((2 * depth,)),
             dma((depth - 1,)),
             dma((depth - 1,)),
             dma((depth - 1,)),
@@ -1295,6 +1358,8 @@
             dma((width, 2)),
             dma((width,)),
             dma((width,)),
+            dma((depth - 1,)),
+            dma((depth - 1,)),
             dma((depth - 1,)),
             dma((depth - 1,)),
             dma((depth, 2)),

time: 96.4 us -> 81.5 us (0.85)
  Pallas kernels: 94.5 us -> 78.9 us
    pallas_call x1, Pallas kernels: 94.5 us -> 78.9 us  [by_heads(): pl.pallas_call(layer_kernel, in_specs=[any_spec] * 11 + [pl.BlockSpec(mem...]
where the time goes in v3:
time: 81.5 us; the launch traced here: 80.6 us
  Pallas kernels  78.9 us (97%)
  local copies, waits for them, and re-layouts  1.67 us (2%)
    pallas_call x1, Pallas kernels, by_heads(): pl.pallas_call(layer_kernel, in_specs=[any_spec] * 11 + [pl.BlockSpec(mem...  78.9 us
    unnamed x1, local copies, waits for them, and re-layouts  1.67 us

profile of v3, /device:TPU:0, one launch (start us, length us, event | category | flops | bytes accessed | tf_op | source)
XLA Modules:
  0.0 80.6 jit_solution(2397255169414916421)
XLA Ops:
  0.0 78.9 %layer.1 = bf16[1,64,2048]{2,1,0:T(8,128)(2,1)} custom-call(bf16[1,128,1024]{2,1,0:T(8,128)(2,1)} %x_ref.1, bf16[128,512]{1,0:T(8,128)(2,1)} %wr_ref.1, bf16[128,512]{1,0:T(8,128)(2,1)} %wk_ref.1, bf16[128,512]{1,0:T(8,128)(2,1)} %wv_ref.1, bf16[128,512]{1,0:T(8,128)(2,1)} %wq_ref.1, f32[1,8,128]{2,1,0:T(8,128)} %extra_ref.1, bf16[2,96,1024]{2,1,0:T(8,128)(2,1)} %dup_ref.1, ...), custom_call_target="tpu_custom_call" | custom-call | tf_op jit(solution)/shard_map/layer/pallas_call | solution.py:1325
  78.9 1.7 %copy.23 = bf16[1,64,2048]{2,1,0:T(8,128)(2,1)} copy(bf16[1,64,2048]{2,1,0:T(8,128)(2,1)} %layer.1) | data formatting | bytes 524288

commit v4 on v3

--- a/solution.py
+++ b/solution.py
@@ -685,6 +685,17 @@
         finish_batch(index, 0)
         hook()
 
+    def norm(place, carry):
+        rows = rows_at(place)
+        lin_sum = s_lin[0, rows, :] + s_lin[1, rows, :]
+        centred = lin_sum - head_sum(lin_sum) * (1.0 / HD)
+        spread = head_sum(centred * centred) * (1.0 / HD)
+        mix_ref[0, rows, :] = (centred * lax.rsqrt(spread + GROUP_EPS) * gain).astype(BF16)
+        return carry
+
+    lax.fori_loop(0, count, norm, 0)
+    hook()
+
     quarter = HD // 4
     back = lax.rem(lane, 2 * quarter) >= quarter
     by_row = lax.rem(lane, HD) < 2 * quarter
@@ -746,23 +757,13 @@
             raised = jnp.exp(scores - top)
             bottom = jnp.exp(sinks[head] - top) + jnp.sum(raised, axis=1, keepdims=True)
             mixed.append(mm((raised / bottom).astype(BF16), held))
-        mix_ref[rows, PAIR:] = jnp.where(mine, mixed[0], mixed[1]).astype(BF16)
+        mix_ref[1, rows, :] = jnp.where(mine, mixed[0], mixed[1]).astype(BF16)
         return carry
 
     blocks = total // ATT_BLOCK
     for part in range(2):
         lax.fori_loop(part * blocks // 2, (part + 1) * blocks // 2, attend, 0)
         hook()
-
-    def norm(place, carry):
-        rows = rows_at(place)
-        lin_sum = s_lin[0, rows, :] + s_lin[1, rows, :]
-        centred = lin_sum - head_sum(lin_sum) * (1.0 / HD)
-        spread = head_sum(centred * centred) * (1.0 / HD)
-        mix_ref[rows, :PAIR] = (centred * lax.rsqrt(spread + GROUP_EPS) * gain).astype(BF16)
-        return carry
-
-    lax.fori_loop(0, count, norm, 0)
 
 
 def mix_scratch(total):
@@ -839,6 +840,8 @@
     mbuf,
     mix_ref,
     lbuf,
+    pbuf,
+    rbuf,
     init,
     local_sem,
     wlocal_sem,
@@ -864,8 +867,8 @@
     op_recv,
     of_send,
     of_recv,
-    os_send,
-    os_recv,
+    part_send,
+    part_recv,
     m_send,
     m_recv,
     *scratch,
@@ -905,7 +908,7 @@
     own_o = [
         pltpu.make_async_copy(
             ref,
-            owb.at[tp, pl.ds(place * out_rows, out_rows), cols_of(sp, fs)],
+            owb.at[pl.ds(place * out_rows, out_rows), cols_of(sp, fs)],
             local_sem.at[1 + place],
         )
         for place, ref in enumerate((lin_ref, win_ref))
@@ -929,8 +932,7 @@
     wbuf[rows_of(sp, fs), lanes(4)] = jnp.where(sp >= 2, packs[1], packs[0])
 
     barrier = pltpu.get_barrier_semaphore()
-    pairs = [(k, t) for k in range(depth) for t in range(sides) if k or t]
-    peers = [{"sp": flipped(sp, k), "tp": tp + t - 2 * t * tp} for k, t in pairs] + [*plane]
+    peers = [{"sp": flipped(sp, k)} for k in range(1, depth)] + [sibling, *plane]
     for peer in peers:
         pl.semaphore_signal(barrier, inc=1, device_id=peer, device_id_type=MESH_IDS)
     pl.semaphore_wait(barrier, len(peers))
@@ -986,7 +988,7 @@
         return remote(there, there, f_send.at[k], f_recv.at[k], plane[side])
 
     def o_move(z, send, recv, device):
-        there = owb.at[tp, :, cols_of(z, fs)]
+        there = owb.at[:, cols_of(z, fs)]
         return remote(there, there, send, recv, device)
 
     def o_up(z, k):
@@ -1001,13 +1003,9 @@
     def of_block(z):
         odd = lax.rem(z, 2)
         near, far = flipped(fs, 1), flipped(fs, 2)
-        there = owb.at[tp, :, cols_of(z, far + odd * (near - far))]
+        there = owb.at[:, cols_of(z, far + odd * (near - far))]
         device = {"fs": near + odd * (far - near)}
         return remote(there, there, of_send.at[z], of_recv.at[z], device)
-
-    def os_block(z):
-        there = owb.at[tp, :, cols_of(z, 0, width)]
-        return remote(there, there, os_send.at[z], os_recv.at[z], sibling)
 
     def x_step(k):
         for part in range(PARTS):
@@ -1034,13 +1032,17 @@
         o_own(k)
 
     def o_own(k):
-        if k < depth - 1:
-
-            @pl.when(sp == k)
+        if k == 0:
+            ups, dns = sp == 0, sp == depth - 1
+        else:
+            ups, dns = (sp > 0) & up_exists, (sp < depth - 1) & dn_exists
+        if k < 2:
+
+            @pl.when(ups)
             def _():
                 o_up(sp, 0).start()
 
-            @pl.when(sp == depth - 1 - k)
+            @pl.when(dns)
             def _():
                 o_dn(sp, 0).start()
 
@@ -1059,41 +1061,61 @@
         for side in range(2):
             op_block(z, side).start()
 
-    def o_step(k):
-        @pl.when(sp >= k)
+    inner = (sp > 0) & up_exists
+    odd = lax.rem(sp, 2)
+    next_z = 1 + odd
+    last_z = (depth - 1) * (1 - odd)
+    far_z = jnp.where(sp < 2, sp + 2, sp - 2)
+
+    def o_step(z):
+        @pl.when(z < sp)
         def _():
-            o_up(sp, k - 1).wait_recv()
-            if k < depth - 1:
-
-                @pl.when(up_exists)
-                def _():
-                    o_up(sp - k, k).start()
-
-        @pl.when(sp < depth - k)
+            o_up(sp, sp - z - 1).wait_recv()
+
+            @pl.when(up_exists)
+            def _():
+                o_up(z, sp - z).start()
+
+        @pl.when(z > sp)
         def _():
-            o_dn(sp, k - 1).wait_recv()
-            if k < depth - 1:
-
-                @pl.when(dn_exists)
-                def _():
-                    o_dn(sp + k, k).start()
-
-        at_distance(k, op_start)
-
-    def of_step(k):
-        def body(z):
-            for side in range(2):
-                op_block(z, side).wait_recv()
-            of_block(z).start()
-
-        at_distance(k, body)
-
-    def os_step(k):
-        def body(z):
-            of_block(z).wait_recv()
-            os_block(z).start()
-
-        at_distance(k, body)
+            o_dn(sp, z - sp - 1).wait_recv()
+
+            @pl.when(dn_exists)
+            def _():
+                o_dn(z, z - sp).start()
+
+        op_start(z)
+
+    def of_step(z):
+        for side in range(2):
+            op_block(z, side).wait_recv()
+        of_block(z).start()
+
+    def phase(step, stage):
+        if stage == 0:
+
+            @pl.when(inner)
+            def _():
+                step(last_z)
+
+        elif stage == 3:
+
+            @pl.when(jnp.logical_not(inner))
+            def _():
+                step(last_z)
+
+        else:
+            step(next_z if stage == 1 else far_z)
+
+    def inner_only(step, z):
+        @pl.when(inner)
+        def _():
+            step(z)
+
+    def ends_only(step, z):
+        @pl.when(jnp.logical_not(inner))
+        def _():
+            step(z)
 
     for k in ORDER:
         target = flipped(sp, k)
@@ -1126,16 +1148,17 @@
         copy.wait()
     o_own(0)
     f_step(0)
+    ends_only(op_start, sp)
     for k in ORDER:
         w_step(k)
     f_step(1)
     f_step(3)
     x_step(1)
     f_step(2)
-    op_start(sp)
+    inner_only(op_start, sp)
+    ends_only(of_step, sp)
     x_step(2)
-    x_step(3)
-    of_step(0)
+    phase(o_step, 0)
     for k in range(depth):
         f_block(k).wait_recv()
     for k in range(1, depth):
@@ -1179,28 +1202,44 @@
             learn = eoff[direction : direction + 1] + mm(learn_low, eup[direction])
             learn_ref[direction, where, :] = jax.nn.sigmoid(learn)
 
-    for k in range(depth):
+    for k in range(depth - 1):
         at_distance(k, block)
-        if k == 1:
-            o_step(1)
+    inner_only(of_step, sp)
+    phase(o_step, 1)
+
+    def m_block(part, k):
+        z = flipped(sp, k)
+        return remote(
+            mix_ref.at[part, pl.ds(pl.multiple_of(z * tokens, tokens), tokens)],
+            mbuf.at[part, sp],
+            m_send.at[part, k - 1],
+            m_recv.at[part, k - 1],
+            {"sp": z},
+        )
+
+    def m_send_part(part):
+        for k in range(1, depth):
+            m_block(part, k).start()
+        mbuf[part, sp] = mix_ref[part, pl.ds(pl.multiple_of(sp * tokens, tokens), tokens), :]
 
     plan = [
-        [],
-        [(os_step, 0), (o_step, 2)],
-        [],
-        [],
-        [],
-        [(of_step, 1), (o_step, 3)],
-        [],
-        [],
-        [(of_step, 2)],
-        [],
+        ((x_step, depth - 1), (inner_only, o_step, far_z), (inner_only, of_step, last_z)),
+        ((at_distance, depth - 1, block), (ends_only, of_step, next_z)),
+        ((ends_only, o_step, far_z),),
+        (),
+        (),
+        ((inner_only, of_step, next_z),),
+        ((ends_only, o_step, last_z),),
+        ((m_send_part, 0),),
+        ((inner_only, of_step, far_z),),
+        ((ends_only, of_step, far_z),),
+        (),
     ]
     queue = iter(plan)
 
     def hook():
-        for step, k in next(queue, ()):
-            step(k)
+        for step, *arguments in next(queue, ()):
+            step(*arguments)
 
     states = jnp.concatenate([init[d, h] for d in range(2) for h in range(2)], axis=1)
     mix_body(
@@ -1216,49 +1255,44 @@
         *scratch,
     )
 
-    def m_block(k, t):
-        z, side = flipped(sp, k), tp + t - 2 * t * tp
-        start = pl.multiple_of((z * sides + side) * share, share)
+    m_send_part(1)
+    ends_only(of_step, last_z)
+    for part in range(2):
+        for k in range(1, depth):
+            m_block(part, k).wait_recv()
+    lbuf[...] = jnp.concatenate(
+        [mbuf[part, z] for part in range(2) for z in range(depth)], axis=1
+    )
+    kept = pl.ds(pl.multiple_of(tp * share, share), share)
+    given = pl.ds(pl.multiple_of((1 - tp) * share, share), share)
+
+    def part_move(z):
         return remote(
-            mix_ref.at[pl.ds(start, share)],
-            mbuf.at[sp * sides + tp],
-            m_send.at[k * sides + t],
-            m_recv.at[k * sides + t],
-            {"sp": z, "tp": side},
+            pbuf.at[z, given], rbuf.at[z], part_send.at[z], part_recv.at[z], sibling
         )
 
-    for k, t in pairs:
-        m_block(k, t).start()
-    mine = sp * sides + tp
-    mbuf[mine] = mix_ref[pl.ds(pl.multiple_of(mine * share, share), share), :]
-    os_step(1)
-    of_step(3)
-    os_step(2)
-    for k, t in pairs:
-        m_block(k, t).wait_recv()
-    lefts = [
-        jnp.concatenate(
-            [mbuf[z * sides + side, :, :PAIR] for z in range(depth)]
-            + [mbuf[z * sides + side, :, PAIR:] for z in range(depth)],
-            axis=1,
-        )
-        for side in range(sides)
-    ]
-    for side in range(sides):
-        lbuf[side] = lefts[side]
-
     def product(z):
-        os_block(z).wait_recv()
-        span = cols_of(z, 0, width)
-        out_ref[0, :, span] = sum(
-            mm(lbuf[side], owb[side, :, span]) for side in range(sides)
-        ).astype(BF16)
-
-    at_distance(0, product)
-    at_distance(1, product)
-    at_distance(2, product)
-    os_step(3)
-    at_distance(3, product)
+        pbuf[z] = mm(lbuf[...], owb[:, cols_of(z, 0, width)])
+        part_move(z).start()
+
+    def arrived(z):
+        of_block(z).wait_recv()
+        product(z)
+
+    def total_of(z):
+        part_move(z).wait_recv()
+        out_ref[0, :, cols_of(z, 0, width)] = (pbuf[z, kept] + rbuf[z]).astype(BF16)
+
+    arrived(sp)
+    phase(arrived, 0)
+    phase(arrived, 1)
+    total_of(sp)
+    phase(total_of, 0)
+    phase(arrived, 2)
+    phase(total_of, 1)
+    phase(arrived, 3)
+    phase(total_of, 2)
+    phase(total_of, 3)
 
     for k in range(depth - 1):
 
@@ -1283,10 +1317,11 @@
             op_block(k, side).wait_send()
         f_block(k).wait_send()
         of_block(k).wait_send()
-        os_block(k).wait_send()
+        part_move(k).wait_send()
         sib_move(k).wait_send()
-    for k, t in pairs:
-        m_block(k, t).wait_send()
+    for part in range(2):
+        for k in range(1, depth):
+            m_block(part, k).wait_send()
 
 
 def by_heads(
@@ -1337,10 +1372,12 @@
             pltpu.VMEM((total, 5 * PAIR), BF16),
             pltpu.VMEM((2, total, PAIR), F32),
             pltpu.VMEM((2, total, PAIR), F32),
-            pltpu.VMEM((sides, 2 * out_rows, features), BF16),
-            pltpu.VMEM((depth * sides, share, 2 * PAIR), BF16),
-            pltpu.VMEM((total, 2 * PAIR), BF16),
-            pltpu.VMEM((sides, share, 2 * out_rows), BF16),
+            pltpu.VMEM((2 * out_rows, features), BF16),
+            pltpu.VMEM((2, depth, tokens, PAIR), BF16),
+            pltpu.VMEM((2, total, PAIR), BF16),
+            pltpu.VMEM((tokens, 2 * out_rows), BF16),
+            pltpu.VMEM((depth, tokens, width * out_cols), F32),
+            pltpu.VMEM((depth, share, width * out_cols), F32),
             pltpu.VMEM((2, 2, HD, HD), F32),
             dma((7,)),
             dma((4,)),
@@ -1368,8 +1405,8 @@
             dma((depth,)),
             dma((depth,)),
             dma((depth,)),
-            dma((depth * sides,)),
-            dma((depth * sides,)),
+            dma((2, depth - 1)),
+            dma((2, depth - 1)),
         ]
         + mix_scratch(total),
         compiler_params=pltpu.CompilerParams(

time: 81.5 us -> 78.3 us (0.961)
  Pallas kernels: 78.9 us -> 76.5 us
    pallas_call x1, Pallas kernels: 78.9 us -> 76.5 us  [by_heads(): pl.pallas_call(layer_kernel, in_specs=[any_spec] * 11 + [pl.BlockSpec(mem...]
where the time goes in v4:
time: 78.3 us; the launch traced here: 78.2 us
  Pallas kernels  76.5 us (98%)
  local copies, waits for them, and re-layouts  1.67 us (2%)
    pallas_call x1, Pallas kernels, by_heads(): pl.pallas_call(layer_kernel, in_specs=[any_spec] * 11 + [pl.BlockSpec(mem...  76.5 us
    unnamed x1, local copies, waits for them, and re-layouts  1.67 us

profile of v4, /device:TPU:0, one launch (start us, length us, event | category | flops | bytes accessed | tf_op | source)
XLA Modules:
  0.0 78.2 jit_solution(5463526218207455187)
XLA Ops:
  0.0 76.5 %layer.1 = bf16[1,64,2048]{2,1,0:T(8,128)(2,1)} custom-call(bf16[1,128,1024]{2,1,0:T(8,128)(2,1)} %x_ref.1, bf16[128,512]{1,0:T(8,128)(2,1)} %wr_ref.1, bf16[128,512]{1,0:T(8,128)(2,1)} %wk_ref.1, bf16[128,512]{1,0:T(8,128)(2,1)} %wv_ref.1, bf16[128,512]{1,0:T(8,128)(2,1)} %wq_ref.1, f32[1,8,128]{2,1,0:T(8,128)} %extra_ref.1, bf16[2,96,1024]{2,1,0:T(8,128)(2,1)} %dup_ref.1, ...), custom_call_target="tpu_custom_call" | custom-call | tf_op jit(solution)/shard_map/layer/pallas_call | solution.py:1360
  76.5 1.7 %copy.23 = bf16[1,64,2048]{2,1,0:T(8,128)(2,1)} copy(bf16[1,64,2048]{2,1,0:T(8,128)(2,1)} %layer.1) | data formatting | bytes 524288

commit v5 on v4

--- a/solution.py
+++ b/solution.py
@@ -1204,8 +1204,10 @@
 
     for k in range(depth - 1):
         at_distance(k, block)
+        if k == 0:
+            ends_only(o_step, next_z)
     inner_only(of_step, sp)
-    phase(o_step, 1)
+    inner_only(o_step, next_z)
 
     def m_block(part, k):
         z = flipped(sp, k)

time: 78.3 us -> 78.8 us (level)
  no operation moved by 1% of the time
where the time goes in v5:
time: 78.8 us; the launch traced here: 78.6 us
  Pallas kernels  77 us (98%)
  local copies, waits for them, and re-layouts  1.67 us (2%)
    pallas_call x1, Pallas kernels, by_heads(): pl.pallas_call(layer_kernel, in_specs=[any_spec] * 11 + [pl.BlockSpec(mem...  77 us
    unnamed x1, local copies, waits for them, and re-layouts  1.67 us

profile of v5, /device:TPU:0, one launch (start us, length us, event | category | flops | bytes accessed | tf_op | source)
XLA Modules:
  0.0 78.6 jit_solution(1738061521782455012)
XLA Ops:
  0.0 77.0 %layer.1 = bf16[1,64,2048]{2,1,0:T(8,128)(2,1)} custom-call(bf16[1,128,1024]{2,1,0:T(8,128)(2,1)} %x_ref.1, bf16[128,512]{1,0:T(8,128)(2,1)} %wr_ref.1, bf16[128,512]{1,0:T(8,128)(2,1)} %wk_ref.1, bf16[128,512]{1,0:T(8,128)(2,1)} %wv_ref.1, bf16[128,512]{1,0:T(8,128)(2,1)} %wq_ref.1, f32[1,8,128]{2,1,0:T(8,128)} %extra_ref.1, bf16[2,96,1024]{2,1,0:T(8,128)(2,1)} %dup_ref.1, ...), custom_call_target="tpu_custom_call" | custom-call | tf_op jit(solution)/shard_map/layer/pallas_call | solution.py:1362
  77.0 1.7 %copy.23 = bf16[1,64,2048]{2,1,0:T(8,128)(2,1)} copy(bf16[1,64,2048]{2,1,0:T(8,128)(2,1)} %layer.1) | data formatting | bytes 524288
